TPU v7x, 32 devices: a whole 2x2x4 slice. The times are simulated.
32 devices in a mesh: sp: 8 (over z, y), dp: 4 (over x, core).
Axes of the slice: x: 2, y: 2, z: 4, core: 2. Of those that a mesh axis runs over, the one named last changes fastest.
Arguments:
- queries: bfloat16 [4, 1024, 2048], P('dp', 'sp'), may hold values from -8 to 8
- keys: bfloat16 [4, 1024, 2048], P('dp', 'sp'), may hold values from -8 to 8
- values: bfloat16 [4, 1024, 2048], P('dp', 'sp'), may hold values from -6 to 6
- proj_weight: bfloat16 [2048, 2048], P('sp'), may hold values from -0.125 to 0.125
- residual: bfloat16 [4, 1024, 2048], P('dp', 'sp'), may hold values from -6 to 6
- norm_gain: float32 [2048], replicated, may hold values from 0.1 to 1.9
- route: int32 [4, 1024, 2], P('dp', 'sp'), may hold values from 0 to 7, all different within a row; in each aligned block of 128 rows (0 to 127, 128 to 255, ..., all dimensions but the last counted through in order) at most 64 rows name the same one
- route_weight: float32 [4, 1024, 2], P('dp', 'sp'), may hold values from 0.1 to 1
- w_gate: bfloat16 [8, 2048, 1024], P('sp'), may hold values from -0.125 to 0.125
- w_up: bfloat16 [8, 2048, 1024], P('sp'), may hold values from -0.125 to 0.125
- w_down: bfloat16 [8, 1024, 2048], P('sp'), may hold values from -0.1875 to 0.1875
Outputs:
- mixed: bfloat16 [4, 1024, 2048], P('dp', 'sp')
Inputs may be any that keep to these rules, and one draw needn't show every extreme that they name: `route`: in the rows of one device no expert is named by more than 64 rows, a bound that some block reaches.
All inputs are finite; a program needn't handle non-finite values.
Results may differ from a plain program's by a relative error of at most 0.013.
Values may be sent and summed in bfloat16 or wider, within the bound.
A program may use at most 128 MiB of HBM per device.

v0:
```python
import functools
import math

import jax
import jax.numpy as jnp
from jax import lax
from jax.experimental import pallas as pl
from jax.experimental.pallas import tpu as pltpu
from jax.sharding import PartitionSpec as P

HEADS = 16


EPS = 1e-06

MESH = pl.DeviceIdType.MESH


def attention_kernel(
    n, m, ny, q_ref, k_ref, v_ref, proj_ref, res_ref, gain_ref, stream_ref, normed_ref,
    qbuf, kbuf, vbuf, wbuf, osend, obuf,
    in_send, in_recv, o_send, o_recv, w_send, w_recv,
):
    me, dp = lax.axis_index("sp"), lax.axis_index("dp")
    nz = n // ny
    z, y = me // ny, lax.rem(me, ny)
    cores = 2
    nx = m // cores
    x, core = dp // cores, lax.rem(dp, cores)
    rows, width = q_ref.shape
    cols = width // n
    head = width // HEADS
    heads_here = cols // head
    wcols = wbuf.shape[3]

    def peer(sp, d):
        return {"sp": sp, "dp": d}

    barrier = pltpu.get_barrier_semaphore()
    for off in range(1, n):
        pl.semaphore_signal(barrier, inc=1, device_id=peer(lax.rem(me + off, n), dp), device_id_type=MESH)
    for off in range(1, m):
        pl.semaphore_signal(barrier, inc=1, device_id=peer(me, lax.rem(dp + off, m)), device_id_type=MESH)
    pl.semaphore_wait(barrier, n - 1 + m - 1)

    def my_cols(d):
        return pl.ds(pl.multiple_of(d * cols, cols), cols)

    def row_block(d):
        return pl.ds(pl.multiple_of(d * rows, rows), rows)

    trio = ((k_ref, kbuf), (q_ref, qbuf), (v_ref, vbuf))

    def in_copy(t, off):
        ref, buf = trio[t]
        to = lax.rem(me + off, n)
        return pltpu.make_async_remote_copy(
            src_ref=ref.at[:, my_cols(to)], dst_ref=buf.at[row_block(me), :],
            send_sem=in_send.at[t, off], recv_sem=in_recv.at[t, off],
            device_id=peer(to, dp), device_id_type=MESH,
        )

    def in_wait(t, off):
        ref, buf = trio[t]
        origin = lax.rem(me - off + n, n)
        pltpu.make_async_remote_copy(
            src_ref=ref.at[:, my_cols(me)], dst_ref=buf.at[row_block(origin), :],
            send_sem=in_send.at[t, off], recv_sem=in_recv.at[t, off],
            device_id=peer(origin, dp), device_id_type=MESH,
        ).wait_recv()

    for t in range(3):
        for off in range(1, n):
            in_copy(t, off).start()

    sent = []

    def w_start(cond, q, i, dev, own=False):
        slot = len(sent)
        source = proj_ref.at[:, pl.ds(pl.multiple_of(q * wcols, wcols), wcols)] if own else wbuf.at[q, i]
        copy = pltpu.make_async_remote_copy(
            src_ref=source, dst_ref=wbuf.at[q, i],
            send_sem=w_send.at[slot], recv_sem=w_recv.at[q, i],
            device_id=dev, device_id_type=MESH,
        )
        sent.append((cond, copy))
        if cond is None:
            copy.start()
        else:
            pl.when(cond)(copy.start)

    def w_wait(cond, q, i):
        copy = pltpu.make_async_remote_copy(
            src_ref=wbuf.at[q, i], dst_ref=wbuf.at[q, i],
            send_sem=w_send.at[0], recv_sem=w_recv.at[q, i],
            device_id=peer(me, lax.rem(dp + 1, m)), device_id_type=MESH,
        )
        if cond is None:
            copy.wait_recv()
        else:
            pl.when(cond)(copy.wait_recv)

    up, down = z + 1 < nz, z > 0
    above, below = jnp.minimum(z + 1, nz - 1) * ny + y, jnp.maximum(z - 1, 0) * ny + y
    other = x * cores + lax.rem(core + 1, cores)
    w_start(up, dp, me, peer(above, dp), True)
    w_start(down, dp, me, peer(below, dp), True)
    for o in range(1, ny):
        w_start(None, dp, me, peer(z * ny + lax.rem(y + o, ny), dp), True)

    for q in range(m):
        wbuf[q, me] = proj_ref[:, q * wcols : (q + 1) * wcols]
    for ref, buf in trio:
        buf[row_block(me), :] = ref[:, my_cols(me)]

    def across(cond, i):
        for o in range(1, nx):
            w_start(cond, dp, i, peer(me, lax.rem(x + o, nx) * cores + core), False)
        w_start(cond, dp, i, peer(me, other), False)

    def column(dz, upward):
        def run():
            far = z - dz if upward else z + dz
            cond = far >= 0 if upward else far < nz
            far = jnp.clip(far, 0, nz - 1)
            i = far * ny + y
            w_wait(cond, dp, i)
            more = jnp.logical_and(cond, up if upward else down)
            if dz < nz - 1:
                w_start(more, dp, i, peer(above if upward else below, dp))
            for o in range(1, ny):
                w_start(cond, dp, i, peer(z * ny + lax.rem(y + o, ny), dp))
            across(cond, i)
        return run

    def side(dz, upward, o):
        def run():
            far = z - dz if upward else z + dz
            cond = (far >= 0 if upward else far < nz) if dz else None
            far = jnp.clip(far, 0, nz - 1)
            i = far * ny + lax.rem(y + o, ny)
            w_wait(cond, dp, i)
            across(cond, i)
        return run

    def beyond(off, o):
        def run():
            i = lax.rem(me + off, n)
            q = lax.rem(x + o, nx) * cores + core
            w_wait(None, q, i)
            w_start(None, q, i, peer(me, other))
        return run

    tasks = [side(0, True, o) for o in range(1, ny)]
    for dz in range(1, nz):
        tasks += [column(dz, True), column(dz, False)]
        tasks += [side(dz, way, o) for o in range(1, ny) for way in (True, False)]
    late = [beyond(off, o) for off in range(1, n) for o in range(1, nx)]

    def o_copy(d):
        return pltpu.make_async_remote_copy(
            src_ref=osend.at[d], dst_ref=obuf.at[me],
            send_sem=o_send.at[d], recv_sem=o_recv.at[me],
            device_id=peer(d, dp), device_id_type=MESH,
        )

    for t in range(3):
        for off in range(1, n):
            in_wait(t, off)

    scale = 1.0 / math.sqrt(head)
    row_id = lax.broadcasted_iota(jnp.int32, (rows, rows), 0)
    col_id = lax.broadcasted_iota(jnp.int32, (rows, rows), 1)
    later = (row_id > col_id).astype(jnp.bfloat16)
    inside = col_id < row_id

    def attend(d):
        for h in range(heads_here):
            lanes = slice(h * head, (h + 1) * head)
            query = qbuf[d * rows : (d + 1) * rows, lanes]
            total = jnp.zeros((rows, head), jnp.float32)
            carry = jnp.zeros((rows, 1), jnp.float32)
            for b in range(d, -1, -1):
                block = slice(b * rows, (b + 1) * rows)
                score = lax.dot_general(
                    query, kbuf[block, lanes], (((1,), (1,)), ((), ())),
                    preferred_element_type=jnp.float32,
                ) * scale
                soft = jnp.maximum(score, 0.0) + jnp.log1p(jnp.exp(-jnp.abs(score)))
                log_sigmoid = score - soft
                if b == d:
                    soft = jnp.where(inside, soft, 0.0)
                high = soft.astype(jnp.bfloat16)
                low = (soft - high.astype(jnp.float32)).astype(jnp.bfloat16)
                suffix = jnp.dot(high, later, preferred_element_type=jnp.float32) + jnp.dot(
                    low, later, preferred_element_type=jnp.float32
                )
                weight = jnp.exp(log_sigmoid - suffix - carry)
                if b == d:
                    weight = jnp.where(inside, weight, 0.0)
                carry = carry + suffix[:, 0:1] + soft[:, 0:1]
                total = total + jnp.dot(
                    weight.astype(jnp.bfloat16), vbuf[block, lanes], preferred_element_type=jnp.float32
                )
            osend[d, :, lanes] = total.astype(jnp.bfloat16)

    done = 0
    for d in range(n):
        attend(d)

        @pl.when(me == d)
        def _():
            obuf[me] = osend[d]

        @pl.when(me != d)
        def _():
            o_copy(d).start()

        share = (d + 1) * len(tasks) // n
        for run in tasks[done:share]:
            run()
        done = share
    for run in late:
        run()
    for off in range(1, n):
        i = lax.rem(me + off, n)
        for x_off in range(nx):
            w_wait(None, lax.rem(x + x_off, nx) * cores + lax.rem(core + 1, cores), i)
    for off in range(1, n):
        origin = lax.rem(me - off + n, n)
        pltpu.make_async_remote_copy(
            src_ref=osend.at[0], dst_ref=obuf.at[origin],
            send_sem=o_send.at[0], recv_sem=o_recv.at[origin],
            device_id=peer(origin, dp), device_id_type=MESH,
        ).wait_recv()

    square = jnp.zeros((rows, 1), jnp.float32)
    attended = jnp.concatenate([obuf[i] for i in range(n)], axis=1)
    for q in range(m):
        part = slice(q * wcols, (q + 1) * wcols)
        weights = wbuf[q].reshape(width, wcols)
        acc = jnp.dot(attended, weights, preferred_element_type=jnp.float32)
        stream = (res_ref[:, part].astype(jnp.float32) + acc).astype(jnp.bfloat16)
        stream_ref[:, part] = stream
        stream = stream.astype(jnp.float32)
        square = square + jnp.sum(stream * stream, axis=1, keepdims=True)
    factor = lax.rsqrt(square / width + EPS)
    for q in range(m):
        part = slice(q * wcols, (q + 1) * wcols)
        normed_ref[:, part] = (
            stream_ref[:, part].astype(jnp.float32) * factor * gain_ref[:, part]
        ).astype(jnp.bfloat16)

    for t in range(3):
        for off in range(1, n):
            in_copy(t, off).wait_send()
    for d in range(n):
        @pl.when(me != d)
        def _():
            o_copy(d).wait_send()
    for cond, copy in sent:
        if cond is None:
            copy.wait_send()
        else:
            pl.when(cond)(copy.wait_send)


def attention(queries, keys, values, proj_weight, residual, norm_gain):
    n, m = lax.axis_size("sp"), lax.axis_size("dp")
    rows, width = queries.shape
    cols = width // n
    ny = 1 << ((n.bit_length() - 1) // 2)
    nz, nx = n // ny, m // 2
    copies = 1 + ny + 2 * nz * (ny + nx + 1) + (2 * nz) * ny * nx + n * nx
    bf16 = jnp.bfloat16
    vmem = pl.BlockSpec(memory_space=pltpu.VMEM)
    return pl.pallas_call(
        functools.partial(attention_kernel, n, m, ny),
        out_shape=[jax.ShapeDtypeStruct((rows, width), bf16)] * 2,
        in_specs=[vmem] * 6,
        out_specs=[vmem] * 2,
        scratch_shapes=[
            pltpu.VMEM((n * rows, cols), bf16),
            pltpu.VMEM((n * rows, cols), bf16),
            pltpu.VMEM((n * rows, cols), bf16),
            pltpu.VMEM((m, n, cols, width // m), bf16),
            pltpu.VMEM((n, rows, cols), bf16),
            pltpu.VMEM((n, rows, cols), bf16),
            pltpu.SemaphoreType.DMA((3, n)),
            pltpu.SemaphoreType.DMA((3, n)),
            pltpu.SemaphoreType.DMA((n,)),
            pltpu.SemaphoreType.DMA((n,)),
            pltpu.SemaphoreType.DMA((copies,)),
            pltpu.SemaphoreType.DMA((m, n)),
        ],
        compiler_params=pltpu.CompilerParams(
            collective_id=0, has_side_effects=True, vmem_limit_bytes=50 * 1024 * 1024
        ),
    )(queries, keys, values, proj_weight, residual, norm_gain.reshape(1, width))


def flipped(number, off, n):
    result = number
    bit = 1
    while bit < n:
        result = result + bit * lax.rem(off // bit, 2) * (1 - 2 * lax.rem(number // bit, 2))
        bit *= 2
    return result


def expert_kernel(
    n, normed_ref, stream_ref, target_ref, flat_ref, share_ref, gate_hbm, up_hbm, down_hbm, out_ref,
    gate_ref, up_ref, down_ref, outgoing, inbox, outbox, back, total,
    load_sem, there_send, there_recv, back_send, back_recv,
):
    me, dp = lax.axis_index("sp"), lax.axis_index("dp")
    rows, width = normed_ref.shape
    capacity = inbox.shape[1]
    pairs = n // 2

    loads = [
        pltpu.make_async_copy(gate_hbm.at[0], gate_ref, load_sem.at[0]),
        pltpu.make_async_copy(up_hbm.at[0], up_ref, load_sem.at[1]),
        pltpu.make_async_copy(down_hbm.at[0], down_ref, load_sem.at[2]),
    ]
    for load in loads:
        load.start()

    barrier = pltpu.get_barrier_semaphore()
    for off in range(1, n):
        pl.semaphore_signal(
            barrier, inc=1, device_id={"sp": lax.rem(me + off, n), "dp": dp}, device_id_type=MESH
        )

    def gathered(expert):
        slot = lax.broadcasted_iota(jnp.int32, (capacity, rows), 0) + expert * capacity
        chosen = jnp.logical_or(flat_ref[0:1, :] == slot, flat_ref[1:2, :] == slot)
        return jnp.dot(
            chosen.astype(jnp.bfloat16), normed_ref[...], preferred_element_type=jnp.float32
        ).astype(jnp.bfloat16)

    def there(off):
        return pltpu.make_async_remote_copy(
            src_ref=outgoing.at[off], dst_ref=inbox.at[off],
            send_sem=there_send.at[off], recv_sem=there_recv.at[off],
            device_id={"sp": flipped(me, off, n), "dp": dp}, device_id_type=MESH,
        )

    def home(off):
        return pltpu.make_async_remote_copy(
            src_ref=outbox.at[off], dst_ref=back.at[off],
            send_sem=back_send.at[off], recv_sem=back_recv.at[off],
            device_id={"sp": flipped(me, off, n), "dp": dp}, device_id_type=MESH,
        )

    pl.semaphore_wait(barrier, n - 1)

    @pl.loop(0, n)
    def _(step):
        pair = lax.rem(pairs - step // 2, pairs)
        off = pair * 2 + 1 - lax.rem(step, 2)
        block = gathered(flipped(me, off, n))

        @pl.when(off > 0)
        def _():
            outgoing[off] = block
            there(off).start()

        @pl.when(off == 0)
        def _():
            inbox[0] = block

    for load in loads:
        load.wait()

    hidden_width = gate_ref.shape[1]
    piece = min(512, hidden_width)

    @pl.loop(0, pairs)
    def _(step):
        pair = lax.rem(pairs - step, pairs)

        @pl.when(pair > 0)
        def _():
            there(pair * 2).wait_recv()

        there(pair * 2 + 1).wait_recv()
        arrived = inbox[pl.ds(pair * 2, 2)].reshape(2 * capacity, width)
        hidden = []
        for first in range(0, hidden_width, piece):
            part = slice(first, first + piece)
            gate = jnp.dot(arrived, gate_ref[:, part], preferred_element_type=jnp.float32)
            upper = jnp.dot(arrived, up_ref[:, part], preferred_element_type=jnp.float32)
            hidden.append((jax.nn.silu(gate) * upper).astype(jnp.bfloat16))
        hidden = jnp.concatenate(hidden, axis=1)
        for first in range(0, width, piece):
            part = slice(first, first + piece)
            result = jnp.dot(hidden, down_ref[:, part], preferred_element_type=jnp.float32)
            outbox[pl.ds(pair * 2, 2), :, part] = result.astype(jnp.bfloat16).reshape(
                2, capacity, piece
            )

        @pl.when(pair > 0)
        def _():
            home(pair * 2).start()

        @pl.when(pair == 0)
        def _():
            back[0] = outbox[0]

        home(pair * 2 + 1).start()

    total[...] = stream_ref[...].astype(jnp.float32)

    @pl.loop(0, pairs)
    def _(step):
        pair = lax.rem(pairs - step, pairs)

        @pl.when(pair > 0)
        def _():
            home(pair * 2).wait_recv()

        home(pair * 2 + 1).wait_recv()
        slot = lax.broadcasted_iota(jnp.int32, (rows, 2 * capacity), 1)
        even, odd = flipped(me, pair * 2, n), flipped(me, pair * 2 + 1, n)
        slot = jnp.where(slot < capacity, slot + even * capacity, slot - capacity + odd * capacity)
        first = (target_ref[:, 0:1] == slot).astype(jnp.bfloat16)
        second = (target_ref[:, 1:2] == slot).astype(jnp.bfloat16)
        for start in range(0, width, piece):
            part = slice(start, start + piece)
            block = back[pl.ds(pair * 2, 2), :, part].reshape(2 * capacity, piece)
            total[:, part] += share_ref[:, 0:1] * jnp.dot(
                first, block, preferred_element_type=jnp.float32
            ) + share_ref[:, 1:2] * jnp.dot(second, block, preferred_element_type=jnp.float32)

    out_ref[...] = total[...].astype(jnp.bfloat16)

    @pl.loop(1, n)
    def _(off):
        there(off).wait_send()
        home(off).wait_send()


def experts(normed, stream, target, share, w_gate, w_up, w_down):
    n = lax.axis_size("sp")
    rows, width = normed.shape
    capacity = 4 * rows // n
    hidden = w_gate.shape[2]
    bf16 = jnp.bfloat16
    vmem = pl.BlockSpec(memory_space=pltpu.VMEM)
    return pl.pallas_call(
        functools.partial(expert_kernel, n),
        out_shape=jax.ShapeDtypeStruct((rows, width), bf16),
        in_specs=[vmem] * 5 + [pl.BlockSpec(memory_space=pl.ANY)] * 3,
        out_specs=vmem,
        scratch_shapes=[
            pltpu.VMEM((width, hidden), bf16),
            pltpu.VMEM((width, hidden), bf16),
            pltpu.VMEM((hidden, width), bf16),
            pltpu.VMEM((n, capacity, width), bf16),
            pltpu.VMEM((n, capacity, width), bf16),
            pltpu.VMEM((n, capacity, width), bf16),
            pltpu.VMEM((n, capacity, width), bf16),
            pltpu.VMEM((rows, width), jnp.float32),
            pltpu.SemaphoreType.DMA((3,)),
            pltpu.SemaphoreType.DMA((n,)),
            pltpu.SemaphoreType.DMA((n,)),
            pltpu.SemaphoreType.DMA((n,)),
            pltpu.SemaphoreType.DMA((n,)),
        ],
        compiler_params=pltpu.CompilerParams(
            collective_id=1, has_side_effects=True, vmem_limit_bytes=50 * 1024 * 1024
        ),
    )(normed, stream, target, target.T, share, w_gate, w_up, w_down)


def body(
    queries,
    keys,
    values,
    proj_weight,
    residual,
    norm_gain,
    route,
    route_weight,
    w_gate,
    w_up,
    w_down,
):
    seq_span = lax.axis_size("sp")
    rows = queries.shape[1]
    width = queries.shape[2]
    stream, normed = attention(
        queries[0], keys[0], values[0], proj_weight, residual[0], norm_gain
    )
    capacity = 4 * rows // seq_span
    chosen = route[0].reshape(rows * 2)
    one_hot = (chosen[:, None] == jnp.arange(seq_span, dtype=jnp.int32)[None, :]).astype(jnp.int32)
    earlier = jnp.cumsum(one_hot, axis=0) - one_hot
    slot = jnp.sum(earlier * one_hot, axis=1)
    target = (chosen * capacity + slot).reshape(rows, 2)
    return experts(normed, stream, target, route_weight[0], w_gate, w_up, w_down)[None]


def solution(mesh):
    return jax.shard_map(
        body,
        mesh=mesh,
        in_specs=(
            P("dp", "sp", None),
            P("dp", "sp", None),
            P("dp", "sp", None),
            P("sp", None),
            P("dp", "sp", None),
            P(),
            P("dp", "sp", None),
            P("dp", "sp", None),
            P("sp", None, None),
            P("sp", None, None),
            P("sp", None, None),
        ),
        out_specs=P("dp", "sp", None),
        check_vma=False,
    )
```

profile of v0, /device:TPU:0, one launch (start us, length us, event | category | flops | bytes accessed | tf_op | source)
XLA Modules:
  0.0 199.5 jit_solution(1986319435659235268)
XLA Ops:
  0.0 0.8 copy.14
  0.8 0.1 eq.29
  0.9 0.1 eq.25
  1.1 0.6 reduce-window.6
  1.7 0.2 slice_reduce_fusion
  1.9 0.1 fusion.1
  2.0 0.1 reduce_sum.12
  2.2 0.1 copy.16
  2.2 0.7 bitcast_add_fusion
  2.9 0.1 copy.18.target_ref
  3.0 0.8 copy.17
  3.8 0.0 copy-start
  3.8 1.0 copy-done
  4.9 0.0 copy-start.1
  4.9 1.0 copy-done.1
  5.9 0.0 copy-start.2
  5.9 1.0 copy-done.2
  7.0 0.0 copy-start.3
  7.0 1.0 copy-done.3
  8.0 0.0 copy-start.4
  8.0 0.7 copy-done.4
  8.7 89.2 %shard_map.109 = (bf16[128,2048]{1,0:T(8,128)(2,1)S(1)}, bf16[128,2048]{1,0:T(8,128)(2,1)S(1)}) custom-call(bf16[128,2048]{1,0:T(8,128)(2,1)S(1)} %bitcast.19, bf16[128,2048]{1,0:T(8,128)(2,1)S(1)} %bitcast.20, bf16[128,2048]{1,0:T(8,128)(2,1)S(1)} %bitcast.21, bf16[256,2048]{1,0:T(8,128)(2,1)} %proj_ref.1, bf16[128,2048]{1,0:T(8,128)(2,1)S(1)} %bitcast.22, ...), custom_call_target="tpu_custom_call" | custom-call | tf_op jit(solution)/shard_map/pallas_call | solution.py:277
  97.9 100.9 %shard_map.110 = bf16[128,2048]{1,0:T(8,128)(2,1)S(1)} custom-call(bf16[128,2048]{1,0:T(8,128)(2,1)S(1)} %get-tuple-element.7.normed_ref, bf16[128,2048]{1,0:T(8,128)(2,1)S(1)} %get-tuple-element.8.stream_ref, s32[128,2]{1,0:T(8,128)S(1)} %copy.18.target_ref, s32[2,128]{1,0:T(2,128)S(1)} %bitcast.24, f32[128,2]{1,0:T(8,128)S(1)} %bitcast.23, ...), custom_call_target="tpu_custom_call" | custom-call | tf_op jit(solution)/shard_map/pallas_call | solution.py:451
  198.7 0.8 copy.20
  (3 shorter events, 0.0 us)
Async XLA Ops:
  3.8 1.0 copy-start
  4.9 1.0 copy-start.1
  5.9 1.0 copy-start.2
  7.0 1.0 copy-start.3
  8.0 0.7 copy-start.4
where the time goes:
time: 200 us
  Pallas kernels  190 us (95%)
  local copies, waits for them, and re-layouts  8.03 us (4%)
    pallas_call x1, Pallas kernels, experts(): pl.pallas_call(functools.partial(expert_kernel, n), out_shape=jax.ShapeDt...  101 us
    pallas_call x1, Pallas kernels, attention(): pl.pallas_call(functools.partial(attention_kernel, n, m, ny), out_shape=[...  89.2 us
    unnamed x13, local copies, waits for them, and re-layouts  7.22 us

commit v1 on v0

v1 whole, which is shorter than its diff:
```python
import functools
import math

import jax
import jax.numpy as jnp
from jax import lax
from jax.experimental import pallas as pl
from jax.experimental.pallas import tpu as pltpu
from jax.sharding import PartitionSpec as P

HEADS = 16


EPS = 1e-06

MESH = pl.DeviceIdType.MESH


def flipped(number, off, n):
    result = number
    bit = 1
    while bit < n:
        result = result + bit * lax.rem(off // bit, 2) * (1 - 2 * lax.rem(number // bit, 2))
        bit *= 2
    return result


def layer_kernel(
    n, m, ny,
    q_hbm, k_hbm, v_hbm, proj_hbm, res_hbm, gain_hbm, route_hbm, share_hbm, gate_hbm, up_hbm, down_hbm,
    out_ref,
    qbuf, kbuf, vbuf, wbuf, osend, obuf, weight_ref, carry_ref, acc, stream_ref, normed_ref,
    res_ref, gain_ref, route_ref, share_ref, info, cols_ref,
    gate_ref, up_ref, down_ref, outgoing, inbox, outbox, back,
    load_sem, own_sem,
    in_send, in_recv, o_send, o_recv, w_send, w_recv, there_send, there_recv, back_send, back_recv,
):
    me, dp = lax.axis_index("sp"), lax.axis_index("dp")
    nz = n // ny
    z, y = me // ny, lax.rem(me, ny)
    cores = 2
    nx = m // cores
    x, core = dp // cores, lax.rem(dp, cores)
    rows, width = stream_ref.shape
    cols = width // n
    head = width // HEADS
    heads_here = cols // head
    wcols = wbuf.shape[3]
    capacity = inbox.shape[1]
    pairs = n // 2
    bf16, f32 = jnp.bfloat16, jnp.float32

    def peer(sp, d):
        return {"sp": sp, "dp": d}

    def my_cols(d):
        return pl.ds(pl.multiple_of(d * cols, cols), cols)

    def row_block(d):
        return pl.ds(pl.multiple_of(d * rows, rows), rows)

    trio = ((k_hbm, kbuf), (q_hbm, qbuf), (v_hbm, vbuf))

    own = [pltpu.make_async_copy(route_hbm, route_ref, own_sem.at[0]),
           pltpu.make_async_copy(share_hbm, share_ref, own_sem.at[1])]
    own += [
        pltpu.make_async_copy(
            proj_hbm.at[:, pl.ds(q * wcols, wcols)], wbuf.at[q, me], own_sem.at[2 + q]
        )
        for q in range(m)
    ]
    own += [
        pltpu.make_async_copy(ref.at[:, my_cols(me)], buf.at[row_block(me), :], own_sem.at[2 + m + t])
        for t, (ref, buf) in enumerate(trio)
    ]
    loads = [
        pltpu.make_async_copy(res_hbm, res_ref, load_sem.at[3]),
        pltpu.make_async_copy(gain_hbm, gain_ref, load_sem.at[4]),
        pltpu.make_async_copy(gate_hbm.at[0], gate_ref, load_sem.at[0]),
        pltpu.make_async_copy(up_hbm.at[0], up_ref, load_sem.at[1]),
        pltpu.make_async_copy(down_hbm.at[0], down_ref, load_sem.at[2]),
    ]
    for copy in own:
        copy.start()

    barrier = pltpu.get_barrier_semaphore()
    for off in range(1, n):
        pl.semaphore_signal(barrier, inc=1, device_id=peer(lax.rem(me + off, n), dp), device_id_type=MESH)
    for off in range(1, m):
        pl.semaphore_signal(barrier, inc=1, device_id=peer(me, lax.rem(dp + off, m)), device_id_type=MESH)
    pl.semaphore_wait(barrier, n - 1 + m - 1)

    def in_copy(t, off):
        ref, buf = trio[t]
        to = lax.rem(me + off, n)
        return pltpu.make_async_remote_copy(
            src_ref=ref.at[:, my_cols(to)], dst_ref=buf.at[row_block(me), :],
            send_sem=in_send.at[t, off], recv_sem=in_recv.at[t, me],
            device_id=peer(to, dp), device_id_type=MESH,
        )

    def in_start(t):
        for off in range(1, n):
            in_copy(t, off).start()

    def in_wait(t, origin):
        ref, buf = trio[t]

        @pl.when(me != origin)
        def _():
            pltpu.make_async_remote_copy(
                src_ref=ref.at[:, my_cols(0)], dst_ref=buf.at[row_block(origin), :],
                send_sem=in_send.at[t, 0], recv_sem=in_recv.at[t, origin],
                device_id=peer(origin, dp), device_id_type=MESH,
            ).wait_recv()

    sent = []

    def w_start(cond, q, i, dev, own=False):
        slot = len(sent)
        source = proj_hbm.at[:, pl.ds(pl.multiple_of(q * wcols, wcols), wcols)] if own else wbuf.at[q, i]
        copy = pltpu.make_async_remote_copy(
            src_ref=source, dst_ref=wbuf.at[q, i],
            send_sem=w_send.at[slot], recv_sem=w_recv.at[q, i],
            device_id=dev, device_id_type=MESH,
        )
        sent.append((cond, copy))
        if cond is None:
            copy.start()
        else:
            pl.when(cond)(copy.start)

    def w_wait(cond, q, i):
        copy = pltpu.make_async_remote_copy(
            src_ref=wbuf.at[q, i], dst_ref=wbuf.at[q, i],
            send_sem=w_send.at[0], recv_sem=w_recv.at[q, i],
            device_id=peer(me, lax.rem(dp + 1, m)), device_id_type=MESH,
        )
        if cond is None:
            copy.wait_recv()
        else:
            pl.when(cond)(copy.wait_recv)

    up, down = z + 1 < nz, z > 0
    above, below = jnp.minimum(z + 1, nz - 1) * ny + y, jnp.maximum(z - 1, 0) * ny + y
    other = x * cores + lax.rem(core + 1, cores)

    def across(cond, i):
        for o in range(1, nx):
            w_start(cond, dp, i, peer(me, lax.rem(x + o, nx) * cores + core), False)
        w_start(cond, dp, i, peer(me, other), False)

    def column(dz, upward):
        far = z - dz if upward else z + dz
        cond = far >= 0 if upward else far < nz
        far = jnp.clip(far, 0, nz - 1)
        i = far * ny + y
        w_wait(cond, dp, i)
        more = jnp.logical_and(cond, up if upward else down)
        if dz < nz - 1:
            w_start(more, dp, i, peer(above if upward else below, dp))
        for o in range(1, ny):
            w_start(cond, dp, i, peer(z * ny + lax.rem(y + o, ny), dp))
        across(cond, i)

    def side(dz, upward, o):
        far = z - dz if upward else z + dz
        cond = (far >= 0 if upward else far < nz) if dz else None
        far = jnp.clip(far, 0, nz - 1)
        i = far * ny + lax.rem(y + o, ny)
        w_wait(cond, dp, i)
        across(cond, i)

    def beyond(off, o):
        i = lax.rem(me + off, n)
        q = lax.rem(x + o, nx) * cores + core
        w_wait(None, q, i)
        w_start(None, q, i, peer(me, other))

    def columns(dz):
        column(dz, True)
        column(dz, False)

    def sides(dz):
        for o in range(1, ny):
            side(dz, True, o)
            if dz:
                side(dz, False, o)

    w_start(up, dp, me, peer(above, dp), True)
    w_start(down, dp, me, peer(below, dp), True)
    for o in range(1, ny):
        w_start(None, dp, me, peer(z * ny + lax.rem(y + o, ny), dp), True)
    in_start(0)
    for load in loads:
        load.start()

    own[0].wait()
    own[1].wait()
    row_id = lax.broadcasted_iota(jnp.int32, (rows, rows), 0)
    col_id = lax.broadcasted_iota(jnp.int32, (rows, rows), 1)
    expert_id = lax.broadcasted_iota(jnp.int32, (n, rows), 0)
    named = [(route_ref[k : k + 1, :] == expert_id).astype(f32) for k in range(2)]
    before = jnp.dot(
        (named[0] + named[1]).astype(bf16), (row_id < col_id).astype(bf16), preferred_element_type=f32
    )
    facts = [
        route_ref[k : k + 1, :].astype(f32) * capacity + jnp.sum(named[k] * before, axis=0, keepdims=True)
        for k in range(2)
    ] + [share_ref[0:1, :], share_ref[1:2, :]]
    for k in range(4):
        info[k : k + 1, :] = facts[k]
    spread = jnp.zeros((rows, rows), f32)
    for k in range(4):
        spread = jnp.where(row_id == k, facts[k], spread)
    cols_ref[...] = spread.T

    sides(0)
    columns(1)
    in_start(1)
    sides(1)
    if nz > 2:
        columns(2)
    in_start(2)
    if nz > 2:
        sides(2)

    scale = math.log2(math.e) / math.sqrt(head)
    later = (row_id > col_id).astype(bf16)
    half = jnp.concatenate([later, jnp.ones((rows, rows), bf16)], axis=1)
    summing = jnp.concatenate([half, half], axis=0)
    log2e = math.log2(math.e)
    chunk = 2 * rows

    for copy in own[2:]:
        copy.wait()

    def weigh(b):
        for h in range(heads_here):
            lanes = slice(h * head, (h + 1) * head)
            key = kbuf[b * rows : (b + 1) * rows, lanes]
            for start in range(b * rows, n * rows, chunk):
                stop = min(start + chunk, n * rows)
                score = lax.dot_general(
                    qbuf[start:stop, lanes], key, (((1,), (1,)), ((), ())), preferred_element_type=f32
                ) * scale
                tail = jnp.log(1.0 + jnp.exp2(-jnp.abs(score))) * log2e
                soft = jnp.maximum(score, 0.0) + tail
                log_sigmoid = jnp.minimum(score, 0.0) - tail
                if start == b * rows:
                    inside = lax.broadcasted_iota(jnp.int32, soft.shape, 1) < lax.broadcasted_iota(
                        jnp.int32, soft.shape, 0
                    )
                    soft = jnp.where(inside, soft, 0.0)
                high = soft.astype(bf16)
                low = (soft - high.astype(f32)).astype(bf16)
                sums = jnp.dot(jnp.concatenate([high, low], axis=1), summing, preferred_element_type=f32)
                part = log_sigmoid - sums[:, :rows]
                fresh = rows if start == b * rows else 0
                if fresh < stop - start:
                    carry = carry_ref[h, start + fresh : stop, :]
                    if fresh:
                        carry = jnp.concatenate([jnp.zeros((fresh, rows), f32), carry], axis=0)
                    part = part - carry
                    total = sums[:, rows:] + carry
                else:
                    total = sums[:, rows:]
                weight = jnp.exp2(part)
                if start == b * rows:
                    weight = jnp.where(inside, weight, 0.0)
                weight_ref[h, start:stop, b * rows : (b + 1) * rows] = weight.astype(bf16)
                if b > 0:
                    carry_ref[h, start:stop, :] = total

    for b in range(n - 1, -1, -1):
        in_wait(0, b)
        in_wait(1, b)
        weigh(b)
    for dz in range(3, nz):
        columns(dz)
        sides(dz)

    def o_copy(d):
        return pltpu.make_async_remote_copy(
            src_ref=osend.at[d], dst_ref=obuf.at[me],
            send_sem=o_send.at[d], recv_sem=o_recv.at[me],
            device_id=peer(d, dp), device_id_type=MESH,
        )

    for d in range(n):
        in_wait(2, d)
        for h in range(heads_here):
            lanes = slice(h * head, (h + 1) * head)
            osend[d, :, lanes] = jnp.dot(
                weight_ref[h, d * rows : (d + 1) * rows, : (d + 1) * rows],
                vbuf[: (d + 1) * rows, lanes],
                preferred_element_type=f32,
            ).astype(bf16)

        @pl.when(me == d)
        def _():
            obuf[me] = osend[d]

        @pl.when(me != d)
        def _():
            o_copy(d).start()

    for off in range(1, n):
        for o in range(1, nx):
            beyond(off, o)
    for off in range(1, n):
        i = lax.rem(me + off, n)
        for x_off in range(nx):
            w_wait(None, lax.rem(x + x_off, nx) * cores + lax.rem(core + 1, cores), i)
    for load in loads:
        load.wait()

    acc[...] = res_ref[...].astype(f32)

    @pl.loop(0, n)
    def _(step):
        origin = flipped(me, step, n)

        @pl.when(step > 0)
        def _():
            pltpu.make_async_remote_copy(
                src_ref=osend.at[0], dst_ref=obuf.at[origin],
                send_sem=o_send.at[0], recv_sem=o_recv.at[origin],
                device_id=peer(origin, dp), device_id_type=MESH,
            ).wait_recv()

        block = obuf[origin]
        for q in range(m):
            part = slice(q * wcols, (q + 1) * wcols)
            acc[:, part] += jnp.dot(block, wbuf[q, origin], preferred_element_type=f32)

    square = jnp.zeros((rows, 1), f32)
    for q in range(m):
        part = slice(q * wcols, (q + 1) * wcols)
        stream = acc[:, part].astype(bf16)
        stream_ref[:, part] = stream
        stream = stream.astype(f32)
        acc[:, part] = stream
        square = square + jnp.sum(stream * stream, axis=1, keepdims=True)
    factor = lax.rsqrt(square / width + EPS)
    for q in range(m):
        part = slice(q * wcols, (q + 1) * wcols)
        normed_ref[:, part] = (acc[:, part] * factor * gain_ref[:, part]).astype(bf16)

    def gathered(expert):
        slot = lax.broadcasted_iota(jnp.int32, (capacity, rows), 0) + expert * capacity
        slot = slot.astype(f32)
        chosen = jnp.logical_or(info[0:1, :] == slot, info[1:2, :] == slot)
        return jnp.dot(chosen.astype(bf16), normed_ref[...], preferred_element_type=f32).astype(bf16)

    def there(off):
        return pltpu.make_async_remote_copy(
            src_ref=outgoing.at[off], dst_ref=inbox.at[off],
            send_sem=there_send.at[off], recv_sem=there_recv.at[off],
            device_id=peer(flipped(me, off, n), dp), device_id_type=MESH,
        )

    def home(off):
        return pltpu.make_async_remote_copy(
            src_ref=outbox.at[off], dst_ref=back.at[off],
            send_sem=back_send.at[off], recv_sem=back_recv.at[off],
            device_id=peer(flipped(me, off, n), dp), device_id_type=MESH,
        )

    @pl.loop(1, n)
    def _(off):
        outgoing[off] = gathered(flipped(me, off, n))
        there(off).start()

    inbox[0] = gathered(me)

    hidden_width = gate_ref.shape[1]
    piece = min(512, hidden_width)

    @pl.loop(0, pairs)
    def _(pair):
        @pl.when(pair > 0)
        def _():
            there(pair * 2).wait_recv()

        there(pair * 2 + 1).wait_recv()
        arrived = inbox[pl.ds(pair * 2, 2)].reshape(2 * capacity, width)
        hidden = []
        for first in range(0, hidden_width, piece):
            part = slice(first, first + piece)
            gate = jnp.dot(arrived, gate_ref[:, part], preferred_element_type=f32)
            upper = jnp.dot(arrived, up_ref[:, part], preferred_element_type=f32)
            hidden.append((jax.nn.silu(gate) * upper).astype(bf16))
        hidden = jnp.concatenate(hidden, axis=1)
        for first in range(0, width, piece):
            part = slice(first, first + piece)
            result = jnp.dot(hidden, down_ref[:, part], preferred_element_type=f32)
            outbox[pl.ds(pair * 2, 2), :, part] = result.astype(bf16).reshape(2, capacity, piece)

        @pl.when(pair > 0)
        def _():
            home(pair * 2).start()

        @pl.when(pair == 0)
        def _():
            back[0] = outbox[0]

        home(pair * 2 + 1).start()

    @pl.loop(0, pairs)
    def _(pair):
        @pl.when(pair > 0)
        def _():
            home(pair * 2).wait_recv()

        home(pair * 2 + 1).wait_recv()
        slot = lax.broadcasted_iota(jnp.int32, (rows, 2 * capacity), 1)
        even, odd = flipped(me, pair * 2, n), flipped(me, pair * 2 + 1, n)
        slot = jnp.where(slot < capacity, slot + even * capacity, slot - capacity + odd * capacity)
        slot = slot.astype(f32)
        first = (cols_ref[:, 0:1] == slot).astype(bf16)
        second = (cols_ref[:, 1:2] == slot).astype(bf16)
        for start in range(0, width, piece):
            part = slice(start, start + piece)
            block = back[pl.ds(pair * 2, 2), :, part].reshape(2 * capacity, piece)
            acc[:, part] += cols_ref[:, 2:3] * jnp.dot(
                first, block, preferred_element_type=f32
            ) + cols_ref[:, 3:4] * jnp.dot(second, block, preferred_element_type=f32)

    out_ref[...] = acc[...].astype(bf16)

    for t in range(3):
        for off in range(1, n):
            in_copy(t, off).wait_send()
    for d in range(n):
        @pl.when(me != d)
        def _():
            o_copy(d).wait_send()
    for cond, copy in sent:
        if cond is None:
            copy.wait_send()
        else:
            pl.when(cond)(copy.wait_send)

    @pl.loop(1, n)
    def _(off):
        there(off).wait_send()
        home(off).wait_send()


def layer(queries, keys, values, proj_weight, residual, norm_gain, route, share, w_gate, w_up, w_down):
    n, m = lax.axis_size("sp"), lax.axis_size("dp")
    rows, width = queries.shape
    cols = width // n
    ny = 1 << ((n.bit_length() - 1) // 2)
    nz, nx = n // ny, m // 2
    copies = 1 + ny + 2 * nz * (ny + nx + 1) + (2 * nz) * ny * nx + n * nx
    capacity = 4 * rows // n
    hidden = w_gate.shape[2]
    heads_here = cols // (width // HEADS)
    bf16, f32 = jnp.bfloat16, jnp.float32
    return pl.pallas_call(
        functools.partial(layer_kernel, n, m, ny),
        out_shape=jax.ShapeDtypeStruct((rows, width), bf16),
        in_specs=[pl.BlockSpec(memory_space=pl.ANY)] * 11,
        out_specs=pl.BlockSpec(memory_space=pltpu.VMEM),
        scratch_shapes=[
            pltpu.VMEM((n * rows, cols), bf16),
            pltpu.VMEM((n * rows, cols), bf16),
            pltpu.VMEM((n * rows, cols), bf16),
            pltpu.VMEM((m, n, cols, width // m), bf16),
            pltpu.VMEM((n, rows, cols), bf16),
            pltpu.VMEM((n, rows, cols), bf16),
            pltpu.VMEM((heads_here, n * rows, n * rows), bf16),
            pltpu.VMEM((heads_here, n * rows, rows), f32),
            pltpu.VMEM((rows, width), f32),
            pltpu.VMEM((rows, width), bf16),
            pltpu.VMEM((rows, width), bf16),
            pltpu.VMEM((rows, width), bf16),
            pltpu.VMEM((1, width), f32),
            pltpu.VMEM((2, rows), jnp.int32),
            pltpu.VMEM((2, rows), f32),
            pltpu.VMEM((8, rows), f32),
            pltpu.VMEM((rows, rows), f32),
            pltpu.VMEM((width, hidden), bf16),
            pltpu.VMEM((width, hidden), bf16),
            pltpu.VMEM((hidden, width), bf16),
            pltpu.VMEM((n, capacity, width), bf16),
            pltpu.VMEM((n, capacity, width), bf16),
            pltpu.VMEM((n, capacity, width), bf16),
            pltpu.VMEM((n, capacity, width), bf16),
            pltpu.SemaphoreType.DMA((5,)),
            pltpu.SemaphoreType.DMA((5 + m,)),
            pltpu.SemaphoreType.DMA((3, n)),
            pltpu.SemaphoreType.DMA((3, n)),
            pltpu.SemaphoreType.DMA((n,)),
            pltpu.SemaphoreType.DMA((n,)),
            pltpu.SemaphoreType.DMA((copies,)),
            pltpu.SemaphoreType.DMA((m, n)),
            pltpu.SemaphoreType.DMA((n,)),
            pltpu.SemaphoreType.DMA((n,)),
            pltpu.SemaphoreType.DMA((n,)),
            pltpu.SemaphoreType.DMA((n,)),
        ],
        compiler_params=pltpu.CompilerParams(
            collective_id=0, has_side_effects=True, vmem_limit_bytes=56 * 1024 * 1024
        ),
    )(
        queries, keys, values, proj_weight, residual, norm_gain.reshape(1, width),
        route.T, share.T, w_gate, w_up, w_down,
    )


def body(
    queries,
    keys,
    values,
    proj_weight,
    residual,
    norm_gain,
    route,
    route_weight,
    w_gate,
    w_up,
    w_down,
):
    return layer(
        queries[0], keys[0], values[0], proj_weight, residual[0], norm_gain,
        route[0], route_weight[0], w_gate, w_up, w_down,
    )[None]


def solution(mesh):
    return jax.shard_map(
        body,
        mesh=mesh,
        in_specs=(
            P("dp", "sp", None),
            P("dp", "sp", None),
            P("dp", "sp", None),
            P("sp", None),
            P("dp", "sp", None),
            P(),
            P("dp", "sp", None),
            P("dp", "sp", None),
            P("sp", None, None),
            P("sp", None, None),
            P("sp", None, None),
        ),
        out_specs=P("dp", "sp", None),
        check_vma=False,
    )
```

time: 200 us -> 167 us (0.83)
  the two profiles are of different devices: /device:TPU:0 before, /device:TPU:20 now
where the time goes in v1:
time: 167 us
  Pallas kernels  165 us (99%)
  local copies, waits for them, and re-layouts  1.88 us (1%)
    pallas_call x1, Pallas kernels, layer(): pl.pallas_call(functools.partial(layer_kernel, n, m, ny), out_shape=jax.S...  165 us

profile of v1, /device:TPU:20, one launch (start us, length us, event | category | flops | bytes accessed | tf_op | source)
XLA Modules:
  0.0 166.7 jit_solution(16239892663389278270)
XLA Ops:
  0.0 164.8 %shard_map.109 = bf16[128,2048]{1,0:T(8,128)(2,1)} custom-call(bf16[128,2048]{1,0:T(8,128)(2,1)} %bitcast.13, bf16[128,2048]{1,0:T(8,128)(2,1)} %bitcast.14, bf16[128,2048]{1,0:T(8,128)(2,1)} %bitcast.15, bf16[256,2048]{1,0:T(8,128)(2,1)} %proj_hbm.1, bf16[128,2048]{1,0:T(8,128)(2,1)} %bitcast.16, f32[1,2048]{1,0:T(1,128)} %bitcast.17, s32[2,128]{1,0:T(2,128)} %bitcast.18, ...), custom_call_target="tpu_custom_call" | custom-call | tf_op jit(solution)/shard_map/pallas_call | solution.py:462
  164.8 1.9 %copy.13 = bf16[1,128,2048]{2,1,0:T(8,128)(2,1)} copy(bf16[1,128,2048]{2,1,0:T(8,128)(2,1)} %bitcast.12) | data formatting | bytes 1048576

commit v2 on v1

--- a/solution.py
+++ b/solution.py
@@ -32,8 +32,10 @@
     qbuf, kbuf, vbuf, wbuf, osend, obuf, weight_ref, carry_ref, acc, stream_ref, normed_ref,
     res_ref, gain_ref, route_ref, share_ref, info, cols_ref,
     gate_ref, up_ref, down_ref, outgoing, inbox, outbox, back,
+    raw_ref, relay_out, relay_in, partial_ref, part_ref, mate_info, mate_cols,
     load_sem, own_sem,
     in_send, in_recv, o_send, o_recv, w_send, w_recv, there_send, there_recv, back_send, back_recv,
+    info_sem, raw_sem, relay_send, via_recv, part_sem,
 ):
     me, dp = lax.axis_index("sp"), lax.axis_index("dp")
     nz = n // ny
@@ -83,6 +85,26 @@
     for copy in own:
         copy.start()
 
+    relayed = nz == 4
+    span = n // 2 if relayed else n
+    edge = jnp.logical_or(z == 0, z == nz - 1)
+    inner = jnp.logical_not(edge) if relayed else me >= 0
+    mate = lax.rem(me + n // 2, n)
+    lumps = raw_sem.shape[1]
+    lump = width // lumps
+    info_copy = pltpu.make_async_remote_copy(
+        src_ref=info, dst_ref=mate_info, send_sem=info_sem.at[0], recv_sem=info_sem.at[1],
+        device_id=peer(mate, dp), device_id_type=MESH,
+    )
+
+    def raw_copy(i):
+        part = slice(i * lump, (i + 1) * lump)
+        return pltpu.make_async_remote_copy(
+            src_ref=normed_ref.at[:, part], dst_ref=raw_ref.at[:, part],
+            send_sem=raw_sem.at[0, i], recv_sem=raw_sem.at[1, i],
+            device_id=peer(mate, dp), device_id_type=MESH,
+        )
+
     barrier = pltpu.get_barrier_semaphore()
     for off in range(1, n):
         pl.semaphore_signal(barrier, inc=1, device_id=peer(lax.rem(me + off, n), dp), device_id_type=MESH)
@@ -191,7 +213,6 @@
     w_start(down, dp, me, peer(below, dp), True)
     for o in range(1, ny):
         w_start(None, dp, me, peer(z * ny + lax.rem(y + o, ny), dp), True)
-    in_start(0)
     for load in loads:
         load.start()
 
@@ -210,20 +231,28 @@
     ] + [share_ref[0:1, :], share_ref[1:2, :]]
     for k in range(4):
         info[k : k + 1, :] = facts[k]
+    info[4:8, :] = jnp.zeros((4, rows), f32)
     spread = jnp.zeros((rows, rows), f32)
     for k in range(4):
         spread = jnp.where(row_id == k, facts[k], spread)
     cols_ref[...] = spread.T
+    if relayed:
+        pl.when(edge)(info_copy.start)
 
     sides(0)
     columns(1)
-    in_start(1)
     sides(1)
     if nz > 2:
         columns(2)
-    in_start(2)
+    in_start(0)
+    in_start(1)
     if nz > 2:
         sides(2)
+    for dz in range(3, nz):
+        columns(dz)
+    in_start(2)
+    for dz in range(3, nz):
+        sides(dz)
 
     scale = math.log2(math.e) / math.sqrt(head)
     later = (row_id > col_id).astype(bf16)
@@ -276,10 +305,6 @@
         in_wait(0, b)
         in_wait(1, b)
         weigh(b)
-    for dz in range(3, nz):
-        columns(dz)
-        sides(dz)
-
     def o_copy(d):
         return pltpu.make_async_remote_copy(
             src_ref=osend.at[d], dst_ref=obuf.at[me],
@@ -347,11 +372,10 @@
         part = slice(q * wcols, (q + 1) * wcols)
         normed_ref[:, part] = (acc[:, part] * factor * gain_ref[:, part]).astype(bf16)
 
-    def gathered(expert):
+    def chosen(facts, expert):
         slot = lax.broadcasted_iota(jnp.int32, (capacity, rows), 0) + expert * capacity
         slot = slot.astype(f32)
-        chosen = jnp.logical_or(info[0:1, :] == slot, info[1:2, :] == slot)
-        return jnp.dot(chosen.astype(bf16), normed_ref[...], preferred_element_type=f32).astype(bf16)
+        return jnp.logical_or(facts[0:1, :] == slot, facts[1:2, :] == slot).astype(bf16)
 
     def there(off):
         return pltpu.make_async_remote_copy(
@@ -360,6 +384,14 @@
             device_id=peer(flipped(me, off, n), dp), device_id_type=MESH,
         )
 
+    def relay(off, i):
+        part = slice(i * lump, (i + 1) * lump)
+        return pltpu.make_async_remote_copy(
+            src_ref=relay_out.at[off, :, part], dst_ref=inbox.at[off + span, :, part],
+            send_sem=relay_send.at[i, off], recv_sem=there_recv.at[off + span],
+            device_id=peer(flipped(me, off, n), dp), device_id_type=MESH,
+        )
+
     def home(off):
         return pltpu.make_async_remote_copy(
             src_ref=outbox.at[off], dst_ref=back.at[off],
@@ -367,27 +399,79 @@
             device_id=peer(flipped(me, off, n), dp), device_id_type=MESH,
         )
 
+    def via(off):
+        return pltpu.make_async_remote_copy(
+            src_ref=outbox.at[off], dst_ref=relay_in.at[off - span],
+            send_sem=back_send.at[off], recv_sem=via_recv.at[off - span],
+            device_id=peer(flipped(me, off - span, n), dp), device_id_type=MESH,
+        )
+
+    def part_copy(i):
+        part = slice(i * piece, (i + 1) * piece)
+        return pltpu.make_async_remote_copy(
+            src_ref=partial_ref.at[:, part], dst_ref=part_ref.at[:, part],
+            send_sem=part_sem.at[0, i], recv_sem=part_sem.at[1, i],
+            device_id=peer(mate, dp), device_id_type=MESH,
+        )
+
+    hidden_width = gate_ref.shape[1]
+    piece = width // part_sem.shape[1]
+    hidden_piece = min(512, hidden_width)
+
+    if relayed:
+        @pl.when(edge)
+        def _():
+            for i in range(lumps):
+                raw_copy(i).start()
+
     @pl.loop(1, n)
     def _(off):
-        outgoing[off] = gathered(flipped(me, off, n))
-        there(off).start()
-
-    inbox[0] = gathered(me)
-
-    hidden_width = gate_ref.shape[1]
-    piece = min(512, hidden_width)
+        @pl.when(jnp.logical_or(inner, off < span))
+        def _():
+            outgoing[off] = jnp.dot(
+                chosen(info, flipped(me, off, n)), normed_ref[...], preferred_element_type=f32
+            ).astype(bf16)
+            there(off).start()
+
+    inbox[0] = jnp.dot(chosen(info, me), normed_ref[...], preferred_element_type=f32).astype(bf16)
 
     @pl.loop(0, pairs)
     def _(pair):
-        @pl.when(pair > 0)
-        def _():
-            there(pair * 2).wait_recv()
-
-        there(pair * 2 + 1).wait_recv()
-        arrived = inbox[pl.ds(pair * 2, 2)].reshape(2 * capacity, width)
+        even, odd = pair * 2, pair * 2 + 1
+        local = even == 0
+        if relayed:
+            local = jnp.logical_or(local, jnp.logical_and(inner, even == span))
+
+            @pl.when(jnp.logical_and(inner, even == span))
+            def _():
+                pltpu.make_async_remote_copy(
+                    src_ref=info, dst_ref=mate_info, send_sem=info_sem.at[0], recv_sem=info_sem.at[1],
+                    device_id=peer(mate, dp), device_id_type=MESH,
+                ).wait_recv()
+                for i in range(lumps):
+                    part = slice(i * lump, (i + 1) * lump)
+                    raw_copy(i).wait_recv()
+                    inbox[span, :, part] = jnp.dot(
+                        chosen(mate_info, me), raw_ref[:, part], preferred_element_type=f32
+                    ).astype(bf16)
+
+                    @pl.loop(1, span)
+                    def _(off):
+                        relay_out[off, :, part] = jnp.dot(
+                            chosen(mate_info, flipped(me, off, n)), raw_ref[:, part],
+                            preferred_element_type=f32,
+                        ).astype(bf16)
+                        relay(off, i).start()
+
+        @pl.when(jnp.logical_not(local))
+        def _():
+            there(even).wait_recv()
+
+        there(odd).wait_recv()
+        arrived = inbox[pl.ds(even, 2)].reshape(2 * capacity, width)
         hidden = []
-        for first in range(0, hidden_width, piece):
-            part = slice(first, first + piece)
+        for first in range(0, hidden_width, hidden_piece):
+            part = slice(first, first + hidden_piece)
             gate = jnp.dot(arrived, gate_ref[:, part], preferred_element_type=f32)
             upper = jnp.dot(arrived, up_ref[:, part], preferred_element_type=f32)
             hidden.append((jax.nn.silu(gate) * upper).astype(bf16))
@@ -395,37 +479,102 @@
         for first in range(0, width, piece):
             part = slice(first, first + piece)
             result = jnp.dot(hidden, down_ref[:, part], preferred_element_type=f32)
-            outbox[pl.ds(pair * 2, 2), :, part] = result.astype(bf16).reshape(2, capacity, piece)
-
-        @pl.when(pair > 0)
-        def _():
-            home(pair * 2).start()
-
-        @pl.when(pair == 0)
+            outbox[pl.ds(even, 2), :, part] = result.astype(bf16).reshape(2, capacity, piece)
+
+        if relayed:
+            side_of = even // ny
+            through = side_of == jnp.where(inner, 2, 3)
+        else:
+            through = even < 0
+        direct = jnp.logical_not(through)
+
+        @pl.when(even == 0)
         def _():
             back[0] = outbox[0]
 
-        home(pair * 2 + 1).start()
-
-    @pl.loop(0, pairs)
-    def _(pair):
-        @pl.when(pair > 0)
-        def _():
-            home(pair * 2).wait_recv()
-
-        home(pair * 2 + 1).wait_recv()
+        @pl.when(jnp.logical_and(direct, even > 0))
+        def _():
+            home(even).start()
+
+        @pl.when(direct)
+        def _():
+            home(odd).start()
+
+        if relayed:
+            @pl.when(jnp.logical_and(through, local))
+            def _():
+                relay_in[0] = outbox[span]
+
+            @pl.when(jnp.logical_and(through, jnp.logical_not(local)))
+            def _():
+                via(even).start()
+
+            @pl.when(through)
+            def _():
+                via(odd).start()
+
+    def picks(facts, even, odd):
         slot = lax.broadcasted_iota(jnp.int32, (rows, 2 * capacity), 1)
-        even, odd = flipped(me, pair * 2, n), flipped(me, pair * 2 + 1, n)
         slot = jnp.where(slot < capacity, slot + even * capacity, slot - capacity + odd * capacity)
         slot = slot.astype(f32)
-        first = (cols_ref[:, 0:1] == slot).astype(bf16)
-        second = (cols_ref[:, 1:2] == slot).astype(bf16)
+        return [(facts[:, k : k + 1] == slot).astype(bf16) for k in range(2)]
+
+    def shared(facts, pick, block):
+        first, second = [jnp.dot(pick[k], block, preferred_element_type=f32) for k in range(2)]
+        return facts[:, 2:3] * first + facts[:, 3:4] * second
+
+    def combine(pair):
+        @pl.when(pair > 0)
+        def _():
+            home(pair * 2).wait_recv()
+
+        home(pair * 2 + 1).wait_recv()
+        pick = picks(cols_ref, flipped(me, pair * 2, n), flipped(me, pair * 2 + 1, n))
         for start in range(0, width, piece):
             part = slice(start, start + piece)
             block = back[pl.ds(pair * 2, 2), :, part].reshape(2 * capacity, piece)
-            acc[:, part] += cols_ref[:, 2:3] * jnp.dot(
-                first, block, preferred_element_type=f32
-            ) + cols_ref[:, 3:4] * jnp.dot(second, block, preferred_element_type=f32)
+            acc[:, part] += shared(cols_ref, pick, block)
+
+    @pl.loop(0, span // 2)
+    def _(pair):
+        combine(pair)
+
+    if relayed:
+        @pl.when(inner)
+        def _():
+            spread = jnp.zeros((rows, rows), f32)
+            for k in range(4):
+                spread = jnp.where(row_id == k, mate_info[k : k + 1, :], spread)
+            mate_cols[...] = spread.T
+
+            @pl.loop(1, span)
+            def _(off):
+                pltpu.make_async_remote_copy(
+                    src_ref=outbox.at[0], dst_ref=relay_in.at[off],
+                    send_sem=back_send.at[0], recv_sem=via_recv.at[off],
+                    device_id=peer(flipped(me, off, n), dp), device_id_type=MESH,
+                ).wait_recv()
+
+            pick = [picks(mate_cols, flipped(me, p * 2, n), flipped(me, p * 2 + 1, n)) for p in range(span // 2)]
+            for i in range(width // piece):
+                part = slice(i * piece, (i + 1) * piece)
+                total = jnp.zeros((rows, piece), f32)
+                for p in range(span // 2):
+                    block = relay_in[p * 2 : p * 2 + 2, :, part].reshape(2 * capacity, piece)
+                    total = total + shared(mate_cols, pick[p], block)
+                partial_ref[:, part] = total.astype(bf16)
+                part_copy(i).start()
+
+            @pl.loop(span // 2, pairs)
+            def _(pair):
+                combine(pair)
+
+        @pl.when(edge)
+        def _():
+            for i in range(width // piece):
+                part = slice(i * piece, (i + 1) * piece)
+                part_copy(i).wait_recv()
+                acc[:, part] += part_ref[:, part].astype(f32)
 
     out_ref[...] = acc[...].astype(bf16)
 
@@ -444,8 +593,30 @@
 
     @pl.loop(1, n)
     def _(off):
-        there(off).wait_send()
-        home(off).wait_send()
+        @pl.when(jnp.logical_or(inner, off < span))
+        def _():
+            there(off).wait_send()
+
+        @pl.when(jnp.logical_or(edge, off != span) if relayed else off > 0)
+        def _():
+            home(off).wait_send()
+
+    if relayed:
+        @pl.when(inner)
+        def _():
+            for i in range(lumps):
+                @pl.loop(1, span)
+                def _(off):
+                    relay(off, i).wait_send()
+
+            for i in range(width // piece):
+                part_copy(i).wait_send()
+
+        @pl.when(edge)
+        def _():
+            info_copy.wait_send()
+            for i in range(lumps):
+                raw_copy(i).wait_send()
 
 
 def layer(queries, keys, values, proj_weight, residual, norm_gain, route, share, w_gate, w_up, w_down):
@@ -489,6 +660,13 @@
             pltpu.VMEM((n, capacity, width), bf16),
             pltpu.VMEM((n, capacity, width), bf16),
             pltpu.VMEM((n, capacity, width), bf16),
+            pltpu.VMEM((rows, width), bf16),
+            pltpu.VMEM((n // 2, capacity, width), bf16),
+            pltpu.VMEM((n // 2, capacity, width), bf16),
+            pltpu.VMEM((rows, width), bf16),
+            pltpu.VMEM((rows, width), bf16),
+            pltpu.VMEM((8, rows), f32),
+            pltpu.VMEM((rows, rows), f32),
             pltpu.SemaphoreType.DMA((5,)),
             pltpu.SemaphoreType.DMA((5 + m,)),
             pltpu.SemaphoreType.DMA((3, n)),
@@ -501,9 +679,14 @@
             pltpu.SemaphoreType.DMA((n,)),
             pltpu.SemaphoreType.DMA((n,)),
             pltpu.SemaphoreType.DMA((n,)),
+            pltpu.SemaphoreType.DMA((2,)),
+            pltpu.SemaphoreType.DMA((2, 2)),
+            pltpu.SemaphoreType.DMA((2, n // 2)),
+            pltpu.SemaphoreType.DMA((n // 2,)),
+            pltpu.SemaphoreType.DMA((2, 4)),
         ],
         compiler_params=pltpu.CompilerParams(
-            collective_id=0, has_side_effects=True, vmem_limit_bytes=56 * 1024 * 1024
+            collective_id=0, has_side_effects=True, vmem_limit_bytes=50 * 1024 * 1024
         ),
     )(
         queries, keys, values, proj_weight, residual, norm_gain.reshape(1, width),

time: 167 us -> 167 us (level)
  the two profiles are of different devices: /device:TPU:20 before, /device:TPU:0 now
where the time goes in v2:
time: 167 us
  Pallas kernels  158 us (95%)
  local copies, waits for them, and re-layouts  8.24 us (5%)
    pallas_call x1, Pallas kernels, layer(): pl.pallas_call(functools.partial(layer_kernel, n, m, ny), out_shape=jax.S...  158 us
    unnamed x17, local copies, waits for them, and re-layouts  8.24 us

profile of v2, /device:TPU:0, one launch (start us, length us, event | category | flops | bytes accessed | tf_op | source)
XLA Modules:
  0.0 166.7 jit_solution(12576518863957271241)
XLA Ops:
  0.0 0.0 copy-start
  0.0 1.2 copy-done
  1.2 0.0 copy-start.1
  1.2 1.0 copy-done.1
  2.3 0.0 copy-start.2
  2.3 1.0 copy-done.2
  3.3 0.0 copy-start.3
  3.3 1.0 copy-done.3
  4.4 0.0 copy-start.4
  4.4 1.0 copy-done.4
  5.4 0.0 copy-start.5
  5.4 0.7 copy-done.5
  6.1 0.0 copy-start.6
  6.1 0.7 copy-done.6
  6.8 0.0 copy-start.7
  6.8 0.7 copy-done.7
  7.5 158.5 %shard_map.109 = bf16[128,2048]{1,0:T(8,128)(2,1)S(1)} custom-call(bf16[128,2048]{1,0:T(8,128)(2,1)S(1)} %bitcast.13, bf16[128,2048]{1,0:T(8,128)(2,1)S(1)} %bitcast.14, bf16[128,2048]{1,0:T(8,128)(2,1)S(1)} %bitcast.15, bf16[256,2048]{1,0:T(8,128)(2,1)S(1)} %copy-done, bf16[128,2048]{1,0:T(8,128)(2,1)S(1)} %bitcast.16, f32[1,2048]{1,0:T(1,128)S(1)} %bitcast.17, ...), custom_call_target="tpu_custom_call" | custom-call | tf_op jit(solution)/shard_map/pallas_call | solution.py:633
  165.9 0.8 copy.13
Async XLA Ops:
  0.0 1.2 copy-start
  1.2 1.0 copy-start.1
  2.3 1.0 copy-start.2
  3.3 1.0 copy-start.3
  4.4 1.0 copy-start.4
  5.4 0.7 copy-start.5
  6.1 0.7 copy-start.6
  6.8 0.7 copy-start.7

commit v3 on v2

--- a/solution.py
+++ b/solution.py
@@ -114,15 +114,15 @@
 
     def in_copy(t, off):
         ref, buf = trio[t]
-        to = lax.rem(me + off, n)
+        to = flipped(me, off, n)
         return pltpu.make_async_remote_copy(
             src_ref=ref.at[:, my_cols(to)], dst_ref=buf.at[row_block(me), :],
             send_sem=in_send.at[t, off], recv_sem=in_recv.at[t, me],
             device_id=peer(to, dp), device_id_type=MESH,
         )
 
-    def in_start(t):
-        for off in range(1, n):
+    def in_start(t, first=1, last=n):
+        for off in range(first, last):
             in_copy(t, off).start()
 
     def in_wait(t, origin):
@@ -213,6 +213,7 @@
     w_start(down, dp, me, peer(below, dp), True)
     for o in range(1, ny):
         w_start(None, dp, me, peer(z * ny + lax.rem(y + o, ny), dp), True)
+    in_start(0, 1, 2 * ny)
     for load in loads:
         load.start()
 
@@ -239,20 +240,16 @@
     if relayed:
         pl.when(edge)(info_copy.start)
 
+    columns(1)
     sides(0)
-    columns(1)
-    sides(1)
+    in_start(0, 2 * ny)
     if nz > 2:
         columns(2)
-    in_start(0)
     in_start(1)
-    if nz > 2:
-        sides(2)
+    in_start(2)
+    sides(1)
     for dz in range(3, nz):
         columns(dz)
-    in_start(2)
-    for dz in range(3, nz):
-        sides(dz)
 
     scale = math.log2(math.e) / math.sqrt(head)
     later = (row_id > col_id).astype(bf16)
@@ -305,6 +302,10 @@
         in_wait(0, b)
         in_wait(1, b)
         weigh(b)
+        if b == n // 2 and nz > 2:
+            sides(2)
+    for dz in range(3, nz):
+        sides(dz)
     def o_copy(d):
         return pltpu.make_async_remote_copy(
             src_ref=osend.at[d], dst_ref=obuf.at[me],
@@ -322,13 +323,11 @@
                 preferred_element_type=f32,
             ).astype(bf16)
 
-        @pl.when(me == d)
-        def _():
-            obuf[me] = osend[d]
-
-        @pl.when(me != d)
-        def _():
-            o_copy(d).start()
+    obuf[me] = osend[me]
+
+    @pl.loop(1, n)
+    def _(off):
+        o_copy(flipped(me, off, n)).start()
 
     for off in range(1, n):
         for o in range(1, nx):
@@ -424,44 +423,55 @@
             for i in range(lumps):
                 raw_copy(i).start()
 
-    @pl.loop(1, n)
+    def pack(off):
+        outgoing[off] = jnp.dot(
+            chosen(info, flipped(me, off, n)), normed_ref[...], preferred_element_type=f32
+        ).astype(bf16)
+
+    @pl.loop(1, span)
     def _(off):
-        @pl.when(jnp.logical_or(inner, off < span))
-        def _():
-            outgoing[off] = jnp.dot(
-                chosen(info, flipped(me, off, n)), normed_ref[...], preferred_element_type=f32
-            ).astype(bf16)
-            there(off).start()
+        pack(off)
+        there(off).start()
 
     inbox[0] = jnp.dot(chosen(info, me), normed_ref[...], preferred_element_type=f32).astype(bf16)
 
+    if relayed:
+        @pl.when(inner)
+        def _():
+            pl.loop(span, n)(pack)
+            info_copy.wait_recv()
+            for i in range(lumps):
+                part = slice(i * lump, (i + 1) * lump)
+                raw_copy(i).wait_recv()
+
+                @pl.loop(1, span)
+                def _(off):
+                    relay_out[off, :, part] = jnp.dot(
+                        chosen(mate_info, flipped(me, off, n)), raw_ref[:, part],
+                        preferred_element_type=f32,
+                    ).astype(bf16)
+                    relay(off, i).start()
+
+                inbox[span, :, part] = jnp.dot(
+                    chosen(mate_info, me), raw_ref[:, part], preferred_element_type=f32
+                ).astype(bf16)
+
+            @pl.loop(0, span)
+            def _(k):
+                there(span + lax.rem(k + span // 2, span)).start()
+
     @pl.loop(0, pairs)
-    def _(pair):
+    def _(step):
+        pair = step
+        if relayed:
+            part_of, rest = step // (ny // 2), lax.rem(step, ny // 2)
+            middle = jnp.where(part_of == 1, 2, jnp.where(part_of == 2, 1, part_of))
+            outer = jnp.where(part_of == 2, 3, jnp.where(part_of == 3, 2, part_of))
+            pair = jnp.where(inner, middle, outer) * (ny // 2) + rest
         even, odd = pair * 2, pair * 2 + 1
         local = even == 0
         if relayed:
             local = jnp.logical_or(local, jnp.logical_and(inner, even == span))
-
-            @pl.when(jnp.logical_and(inner, even == span))
-            def _():
-                pltpu.make_async_remote_copy(
-                    src_ref=info, dst_ref=mate_info, send_sem=info_sem.at[0], recv_sem=info_sem.at[1],
-                    device_id=peer(mate, dp), device_id_type=MESH,
-                ).wait_recv()
-                for i in range(lumps):
-                    part = slice(i * lump, (i + 1) * lump)
-                    raw_copy(i).wait_recv()
-                    inbox[span, :, part] = jnp.dot(
-                        chosen(mate_info, me), raw_ref[:, part], preferred_element_type=f32
-                    ).astype(bf16)
-
-                    @pl.loop(1, span)
-                    def _(off):
-                        relay_out[off, :, part] = jnp.dot(
-                            chosen(mate_info, flipped(me, off, n)), raw_ref[:, part],
-                            preferred_element_type=f32,
-                        ).astype(bf16)
-                        relay(off, i).start()
 
         @pl.when(jnp.logical_not(local))
         def _():
@@ -581,10 +591,10 @@
     for t in range(3):
         for off in range(1, n):
             in_copy(t, off).wait_send()
-    for d in range(n):
-        @pl.when(me != d)
-        def _():
-            o_copy(d).wait_send()
+    @pl.loop(1, n)
+    def _(off):
+        o_copy(flipped(me, off, n)).wait_send()
+
     for cond, copy in sent:
         if cond is None:
             copy.wait_send()

time: 167 us -> 148 us (0.89)
  Pallas kernels: 158 us -> 139 us
    pallas_call x1, Pallas kernels: 158 us -> 139 us  [layer(): pl.pallas_call(functools.partial(layer_kernel, n, m, ny), out_shape=jax.S...]
where the time goes in v3:
time: 148 us; the launch traced here: 147 us
  Pallas kernels  139 us (94%)
  local copies, waits for them, and re-layouts  8.24 us (6%)
    pallas_call x1, Pallas kernels, layer(): pl.pallas_call(functools.partial(layer_kernel, n, m, ny), out_shape=jax.S...  139 us
    unnamed x17, local copies, waits for them, and re-layouts  8.24 us

profile of v3, /device:TPU:0, one launch (start us, length us, event | category | flops | bytes accessed | tf_op | source)
XLA Modules:
  0.0 147.5 jit_solution(11954207676391995161)
XLA Ops:
  0.0 0.0 copy-start
  0.0 1.2 copy-done
  1.2 0.0 copy-start.1
  1.2 1.0 copy-done.1
  2.3 0.0 copy-start.2
  2.3 1.0 copy-done.2
  3.3 0.0 copy-start.3
  3.3 1.0 copy-done.3
  4.4 0.0 copy-start.4
  4.4 1.0 copy-done.4
  5.4 0.0 copy-start.5
  5.4 0.7 copy-done.5
  6.1 0.0 copy-start.6
  6.1 0.7 copy-done.6
  6.8 0.0 copy-start.7
  6.8 0.7 copy-done.7
  7.5 139.2 %shard_map.109 = bf16[128,2048]{1,0:T(8,128)(2,1)S(1)} custom-call(bf16[128,2048]{1,0:T(8,128)(2,1)S(1)} %bitcast.13, bf16[128,2048]{1,0:T(8,128)(2,1)S(1)} %bitcast.14, bf16[128,2048]{1,0:T(8,128)(2,1)S(1)} %bitcast.15, bf16[256,2048]{1,0:T(8,128)(2,1)S(1)} %copy-done, bf16[128,2048]{1,0:T(8,128)(2,1)S(1)} %bitcast.16, f32[1,2048]{1,0:T(1,128)S(1)} %bitcast.17, ...), custom_call_target="tpu_custom_call" | custom-call | tf_op jit(solution)/shard_map/pallas_call | solution.py:643
  146.7 0.8 copy.13
Async XLA Ops:
  0.0 1.2 copy-start
  1.2 1.0 copy-start.1
  2.3 1.0 copy-start.2
  3.3 1.0 copy-start.3
  4.4 1.0 copy-start.4
  5.4 0.7 copy-start.5
  6.1 0.7 copy-start.6
  6.8 0.7 copy-start.7

commit v4 on v1

--- a/solution.py
+++ b/solution.py
@@ -32,8 +32,10 @@
     qbuf, kbuf, vbuf, wbuf, osend, obuf, weight_ref, carry_ref, acc, stream_ref, normed_ref,
     res_ref, gain_ref, route_ref, share_ref, info, cols_ref,
     gate_ref, up_ref, down_ref, outgoing, inbox, outbox, back,
+    raw_ref, relay_out, relay_in, partial_ref, part_ref, mate_info, mate_cols,
     load_sem, own_sem,
     in_send, in_recv, o_send, o_recv, w_send, w_recv, there_send, there_recv, back_send, back_recv,
+    info_send, info_recv, raw_send, raw_recv, relay_send, via_recv, part_send, part_recv,
 ):
     me, dp = lax.axis_index("sp"), lax.axis_index("dp")
     nz = n // ny
@@ -83,6 +85,30 @@
     for copy in own:
         copy.start()
 
+    half = nz // 2
+    span = half * ny
+    edge = jnp.logical_or(z == 0, z == nz - 1)
+    inner = jnp.logical_not(edge)
+    slot_of = [half * ny, (nz - 1) * ny]
+    my_slot = jnp.where(edge, 0, 1)
+    mate = jnp.where(edge, flipped(me, slot_of[0], n), flipped(me, slot_of[1], n))
+    lumps = raw_send.shape[0]
+    lump = width // lumps
+
+    def info_copy(slot):
+        return pltpu.make_async_remote_copy(
+            src_ref=info, dst_ref=mate_info.at[slot], send_sem=info_send.at[0], recv_sem=info_recv.at[slot],
+            device_id=peer(mate, dp), device_id_type=MESH,
+        )
+
+    def raw_copy(slot, i):
+        part = slice(i * lump, (i + 1) * lump)
+        return pltpu.make_async_remote_copy(
+            src_ref=normed_ref.at[:, part], dst_ref=raw_ref.at[slot, :, part],
+            send_sem=raw_send.at[i], recv_sem=raw_recv.at[slot, i],
+            device_id=peer(mate, dp), device_id_type=MESH,
+        )
+
     barrier = pltpu.get_barrier_semaphore()
     for off in range(1, n):
         pl.semaphore_signal(barrier, inc=1, device_id=peer(lax.rem(me + off, n), dp), device_id_type=MESH)
@@ -92,15 +118,15 @@
 
     def in_copy(t, off):
         ref, buf = trio[t]
-        to = lax.rem(me + off, n)
+        to = flipped(me, off, n)
         return pltpu.make_async_remote_copy(
             src_ref=ref.at[:, my_cols(to)], dst_ref=buf.at[row_block(me), :],
             send_sem=in_send.at[t, off], recv_sem=in_recv.at[t, me],
             device_id=peer(to, dp), device_id_type=MESH,
         )
 
-    def in_start(t):
-        for off in range(1, n):
+    def in_start(t, first=1, last=n):
+        for off in range(first, last):
             in_copy(t, off).start()
 
     def in_wait(t, origin):
@@ -191,7 +217,7 @@
     w_start(down, dp, me, peer(below, dp), True)
     for o in range(1, ny):
         w_start(None, dp, me, peer(z * ny + lax.rem(y + o, ny), dp), True)
-    in_start(0)
+    in_start(0, 1, 2 * ny)
     for load in loads:
         load.start()
 
@@ -210,25 +236,28 @@
     ] + [share_ref[0:1, :], share_ref[1:2, :]]
     for k in range(4):
         info[k : k + 1, :] = facts[k]
+    info[4:8, :] = jnp.zeros((4, rows), f32)
     spread = jnp.zeros((rows, rows), f32)
     for k in range(4):
         spread = jnp.where(row_id == k, facts[k], spread)
     cols_ref[...] = spread.T
-
+    info_copy(my_slot).start()
+
+    columns(1)
     sides(0)
-    columns(1)
-    in_start(1)
-    sides(1)
+    in_start(0, 2 * ny)
     if nz > 2:
         columns(2)
+    in_start(1)
     in_start(2)
-    if nz > 2:
-        sides(2)
+    sides(1)
+    for dz in range(3, nz):
+        columns(dz)
 
     scale = math.log2(math.e) / math.sqrt(head)
     later = (row_id > col_id).astype(bf16)
-    half = jnp.concatenate([later, jnp.ones((rows, rows), bf16)], axis=1)
-    summing = jnp.concatenate([half, half], axis=0)
+    later_all = jnp.concatenate([later, jnp.ones((rows, rows), bf16)], axis=1)
+    summing = jnp.concatenate([later_all, later_all], axis=0)
     log2e = math.log2(math.e)
     chunk = 2 * rows
 
@@ -276,10 +305,10 @@
         in_wait(0, b)
         in_wait(1, b)
         weigh(b)
+        if b == n // 2 and nz > 2:
+            sides(2)
     for dz in range(3, nz):
-        columns(dz)
         sides(dz)
-
     def o_copy(d):
         return pltpu.make_async_remote_copy(
             src_ref=osend.at[d], dst_ref=obuf.at[me],
@@ -297,13 +326,11 @@
                 preferred_element_type=f32,
             ).astype(bf16)
 
-        @pl.when(me == d)
-        def _():
-            obuf[me] = osend[d]
-
-        @pl.when(me != d)
-        def _():
-            o_copy(d).start()
+    obuf[me] = osend[me]
+
+    @pl.loop(1, n)
+    def _(off):
+        o_copy(flipped(me, off, n)).start()
 
     for off in range(1, n):
         for o in range(1, nx):
@@ -347,11 +374,10 @@
         part = slice(q * wcols, (q + 1) * wcols)
         normed_ref[:, part] = (acc[:, part] * factor * gain_ref[:, part]).astype(bf16)
 
-    def gathered(expert):
+    def chosen(facts, expert):
         slot = lax.broadcasted_iota(jnp.int32, (capacity, rows), 0) + expert * capacity
         slot = slot.astype(f32)
-        chosen = jnp.logical_or(info[0:1, :] == slot, info[1:2, :] == slot)
-        return jnp.dot(chosen.astype(bf16), normed_ref[...], preferred_element_type=f32).astype(bf16)
+        return jnp.logical_or(facts[0:1, :] == slot, facts[1:2, :] == slot).astype(bf16)
 
     def there(off):
         return pltpu.make_async_remote_copy(
@@ -360,6 +386,22 @@
             device_id=peer(flipped(me, off, n), dp), device_id_type=MESH,
         )
 
+    def arrival(off):
+        return pltpu.make_async_remote_copy(
+            src_ref=outgoing.at[0], dst_ref=inbox.at[off],
+            send_sem=there_send.at[0], recv_sem=there_recv.at[off],
+            device_id=peer(mate, dp), device_id_type=MESH,
+        )
+
+    def relay(slot, off, i):
+        part = slice(i * lump, (i + 1) * lump)
+        index = flipped(off, slot_of[slot], n)
+        return pltpu.make_async_remote_copy(
+            src_ref=relay_out.at[slot, off, :, part], dst_ref=inbox.at[index, :, part],
+            send_sem=relay_send.at[slot, i, off], recv_sem=there_recv.at[index],
+            device_id=peer(flipped(me, off, n), dp), device_id_type=MESH,
+        )
+
     def home(off):
         return pltpu.make_async_remote_copy(
             src_ref=outbox.at[off], dst_ref=back.at[off],
@@ -367,27 +409,101 @@
             device_id=peer(flipped(me, off, n), dp), device_id_type=MESH,
         )
 
-    @pl.loop(1, n)
-    def _(off):
-        outgoing[off] = gathered(flipped(me, off, n))
+    hidden_width = gate_ref.shape[1]
+    pieces = part_send.shape[1]
+    piece = width // pieces
+    hidden_piece = min(512, hidden_width)
+
+    def via(off, slot, to, i):
+        part = slice(i * piece, (i + 1) * piece)
+        return pltpu.make_async_remote_copy(
+            src_ref=outbox.at[off, :, part], dst_ref=relay_in.at[slot, to, :, part],
+            send_sem=back_send.at[off], recv_sem=via_recv.at[slot, to, i],
+            device_id=peer(flipped(me, to, n), dp), device_id_type=MESH,
+        )
+
+    def part_copy(slot, i):
+        part = slice(i * piece, (i + 1) * piece)
+        return pltpu.make_async_remote_copy(
+            src_ref=partial_ref.at[slot, :, part], dst_ref=part_ref.at[:, part],
+            send_sem=part_send.at[slot, i], recv_sem=part_recv.at[i],
+            device_id=peer(flipped(me, slot_of[slot], n), dp), device_id_type=MESH,
+        )
+
+    def pack(off):
+        outgoing[off] = jnp.dot(
+            chosen(info, flipped(me, off, n)), normed_ref[...], preferred_element_type=f32
+        ).astype(bf16)
         there(off).start()
 
-    inbox[0] = gathered(me)
-
-    hidden_width = gate_ref.shape[1]
-    piece = min(512, hidden_width)
+    def pass_on(slot, chunks):
+        if chunks[0] == 0:
+            info_copy(slot).wait_recv()
+        for i in chunks:
+            part = slice(i * lump, (i + 1) * lump)
+            raw_copy(slot, i).wait_recv()
+
+            @pl.loop(1, span)
+            def _(step):
+                off = span - step
+                relay_out[slot, off, :, part] = jnp.dot(
+                    chosen(mate_info.at[slot], flipped(me, off, n)), raw_ref[slot, :, part],
+                    preferred_element_type=f32,
+                ).astype(bf16)
+                relay(slot, off, i).start()
+
+            inbox[slot_of[slot], :, part] = jnp.dot(
+                chosen(mate_info.at[slot], me), raw_ref[slot, :, part], preferred_element_type=f32
+            ).astype(bf16)
+
+    @pl.when(inner)
+    def _():
+        for i in range(lumps):
+            raw_copy(1, i).start()
+
+    pl.loop(1, span)(pack)
+
+    @pl.when(edge)
+    def _():
+        for i in range(lumps):
+            raw_copy(0, i).start()
+
+    inbox[0] = jnp.dot(chosen(info, me), normed_ref[...], preferred_element_type=f32).astype(bf16)
+
+    @pl.when(inner)
+    def _():
+        pass_on(1, range(1))
 
     @pl.loop(0, pairs)
-    def _(pair):
-        @pl.when(pair > 0)
-        def _():
-            there(pair * 2).wait_recv()
-
-        there(pair * 2 + 1).wait_recv()
-        arrived = inbox[pl.ds(pair * 2, 2)].reshape(2 * capacity, width)
+    def _(step):
+        part_of, rest = step // (ny // 2), lax.rem(step, ny // 2)
+        swapped = jnp.where(part_of == 2, 3, jnp.where(part_of == 3, 2, part_of))
+        part_of = jnp.where(inner, swapped, part_of)
+        even = part_of * ny + rest * 2
+        odd = even + 1
+        far = part_of >= half
+        local = jnp.logical_or(even == 0, jnp.logical_and(inner, jnp.logical_and(far, rest == 0)))
+
+        @pl.when(jnp.logical_and(inner, step == pairs // 4))
+        def _():
+            pass_on(1, range(1, lumps - 1))
+
+        @pl.when(jnp.logical_and(inner, step == pairs // 2))
+        def _():
+            pass_on(1, range(lumps - 1, lumps))
+            pass_on(0, range(lumps))
+            for off in range(ny, span):
+                home(off).start()
+
+        @pl.when(jnp.logical_not(local))
+        def _():
+            arrival(even).wait_recv()
+
+        arrival(odd).wait_recv()
+        arrived = inbox[pl.ds(even, 2)].reshape(2 * capacity, width)
         hidden = []
-        for first in range(0, hidden_width, piece):
-            part = slice(first, first + piece)
+        for first in range(0, hidden_width, hidden_piece):
+            part = slice(first, first + hidden_piece)
             gate = jnp.dot(arrived, gate_ref[:, part], preferred_element_type=f32)
             upper = jnp.dot(arrived, up_ref[:, part], preferred_element_type=f32)
             hidden.append((jax.nn.silu(gate) * upper).astype(bf16))
@@ -395,57 +511,132 @@
         for first in range(0, width, piece):
             part = slice(first, first + piece)
             result = jnp.dot(hidden, down_ref[:, part], preferred_element_type=f32)
-            outbox[pl.ds(pair * 2, 2), :, part] = result.astype(bf16).reshape(2, capacity, piece)
-
-        @pl.when(pair > 0)
-        def _():
-            home(pair * 2).start()
-
-        @pl.when(pair == 0)
+            outbox[pl.ds(even, 2), :, part] = result.astype(bf16).reshape(2, capacity, piece)
+
+        @pl.when(even == 0)
         def _():
             back[0] = outbox[0]
 
-        home(pair * 2 + 1).start()
-
-    @pl.loop(0, pairs)
+        held = jnp.logical_and(inner, part_of == 1)
+
+        @pl.when(jnp.logical_not(jnp.logical_or(far, held)))
+        def _():
+            @pl.when(even > 0)
+            def _():
+                home(even).start()
+
+            home(odd).start()
+
+        @pl.when(far)
+        def _():
+            slot = jnp.where(inner, part_of - half, nz - 1 - part_of)
+            to = jnp.where(inner, 0, ny) + rest * 2
+
+            @pl.when(local)
+            def _():
+                relay_in[slot, 0] = outbox[even]
+
+            for i in range(pieces):
+                @pl.when(jnp.logical_not(local))
+                def _():
+                    via(even, slot, to, i).start()
+
+                via(odd, slot, to + 1, i).start()
+
+    def picks(facts, even, odd):
+        slot = lax.broadcasted_iota(jnp.int32, (rows, 2 * capacity), 1)
+        slot = jnp.where(slot < capacity, slot + even * capacity, slot - capacity + odd * capacity)
+        slot = slot.astype(f32)
+        return [(facts[:, k : k + 1] == slot).astype(bf16) for k in range(2)]
+
+    def shared(facts, pick, block):
+        first, second = [jnp.dot(pick[k], block, preferred_element_type=f32) for k in range(2)]
+        return facts[:, 2:3] * first + facts[:, 3:4] * second
+
+    @pl.loop(0, span // 2)
     def _(pair):
         @pl.when(pair > 0)
         def _():
             home(pair * 2).wait_recv()
 
         home(pair * 2 + 1).wait_recv()
-        slot = lax.broadcasted_iota(jnp.int32, (rows, 2 * capacity), 1)
-        even, odd = flipped(me, pair * 2, n), flipped(me, pair * 2 + 1, n)
-        slot = jnp.where(slot < capacity, slot + even * capacity, slot - capacity + odd * capacity)
-        slot = slot.astype(f32)
-        first = (cols_ref[:, 0:1] == slot).astype(bf16)
-        second = (cols_ref[:, 1:2] == slot).astype(bf16)
+        pick = picks(cols_ref, flipped(me, pair * 2, n), flipped(me, pair * 2 + 1, n))
         for start in range(0, width, piece):
             part = slice(start, start + piece)
             block = back[pl.ds(pair * 2, 2), :, part].reshape(2 * capacity, piece)
-            acc[:, part] += cols_ref[:, 2:3] * jnp.dot(
-                first, block, preferred_element_type=f32
-            ) + cols_ref[:, 3:4] * jnp.dot(second, block, preferred_element_type=f32)
+            acc[:, part] += shared(cols_ref, pick, block)
+
+    @pl.when(inner)
+    def _():
+        for slot in (1, 0):
+            spread = jnp.zeros((rows, rows), f32)
+            for k in range(4):
+                spread = jnp.where(row_id == k, mate_info[slot, k : k + 1, :], spread)
+            mate_cols[slot] = spread.T
+            facts = mate_cols.at[slot]
+            pick = [picks(facts, flipped(me, p * 2, n), flipped(me, p * 2 + 1, n)) for p in range(span // 2)]
+            for i in range(pieces):
+                part = slice(i * piece, (i + 1) * piece)
+
+                @pl.loop(1, span)
+                def _(to):
+                    via(0, slot, to, i).wait_recv()
+
+                total = jnp.zeros((rows, piece), f32)
+                for p in range(span // 2):
+                    block = relay_in[slot, p * 2 : p * 2 + 2, :, part].reshape(2 * capacity, piece)
+                    total = total + shared(facts, pick[p], block)
+                partial_ref[slot, :, part] = total.astype(bf16)
+                part_copy(slot, i).start()
+
+    for i in range(pieces):
+        part = slice(i * piece, (i + 1) * piece)
+        part_copy(0, i).wait_recv()
+        acc[:, part] += part_ref[:, part].astype(f32)
 
     out_ref[...] = acc[...].astype(bf16)
 
     for t in range(3):
         for off in range(1, n):
             in_copy(t, off).wait_send()
-    for d in range(n):
-        @pl.when(me != d)
-        def _():
-            o_copy(d).wait_send()
+    @pl.loop(1, n)
+    def _(off):
+        o_copy(flipped(me, off, n)).wait_send()
+
     for cond, copy in sent:
         if cond is None:
             copy.wait_send()
         else:
             pl.when(cond)(copy.wait_send)
 
+    info_copy(my_slot).wait_send()
+    for i in range(lumps):
+        raw_copy(my_slot, i).wait_send()
+
+    @pl.loop(1, span)
+    def _(off):
+        there(off).wait_send()
+
     @pl.loop(1, n)
     def _(off):
-        there(off).wait_send()
-        home(off).wait_send()
+        @pl.when(jnp.logical_or(edge, jnp.logical_and(off != slot_of[0], off != slot_of[1])))
+        def _():
+            pltpu.make_async_remote_copy(
+                src_ref=outbox.at[off], dst_ref=inbox.at[off],
+                send_sem=back_send.at[off], recv_sem=there_recv.at[off],
+                device_id=peer(mate, dp), device_id_type=MESH,
+            ).wait_send()
+
+    @pl.when(inner)
+    def _():
+        for slot in range(2):
+            for i in range(lumps):
+                @pl.loop(1, span)
+                def _(off):
+                    relay(slot, off, i).wait_send()
+
+            for i in range(pieces):
+                part_copy(slot, i).wait_send()
 
 
 def layer(queries, keys, values, proj_weight, residual, norm_gain, route, share, w_gate, w_up, w_down):
@@ -459,6 +650,7 @@
     hidden = w_gate.shape[2]
     heads_here = cols // (width // HEADS)
     bf16, f32 = jnp.bfloat16, jnp.float32
+    lumps = 4
     return pl.pallas_call(
         functools.partial(layer_kernel, n, m, ny),
         out_shape=jax.ShapeDtypeStruct((rows, width), bf16),
@@ -485,10 +677,17 @@
             pltpu.VMEM((width, hidden), bf16),
             pltpu.VMEM((width, hidden), bf16),
             pltpu.VMEM((hidden, width), bf16),
+            pltpu.VMEM((n // 2, capacity, width), bf16),
             pltpu.VMEM((n, capacity, width), bf16),
             pltpu.VMEM((n, capacity, width), bf16),
-            pltpu.VMEM((n, capacity, width), bf16),
-            pltpu.VMEM((n, capacity, width), bf16),
+            pltpu.VMEM((n // 2, capacity, width), bf16),
+            pltpu.VMEM((2, rows, width), bf16),
+            pltpu.VMEM((2, n // 2, capacity, width), bf16),
+            pltpu.VMEM((2, n // 2, capacity, width), bf16),
+            pltpu.VMEM((2, rows, width), bf16),
+            pltpu.VMEM((rows, width), bf16),
+            pltpu.VMEM((2, 8, rows), f32),
+            pltpu.VMEM((2, rows, rows), f32),
             pltpu.SemaphoreType.DMA((5,)),
             pltpu.SemaphoreType.DMA((5 + m,)),
             pltpu.SemaphoreType.DMA((3, n)),
@@ -501,9 +700,17 @@
             pltpu.SemaphoreType.DMA((n,)),
             pltpu.SemaphoreType.DMA((n,)),
             pltpu.SemaphoreType.DMA((n,)),
+            pltpu.SemaphoreType.DMA((1,)),
+            pltpu.SemaphoreType.DMA((2,)),
+            pltpu.SemaphoreType.DMA((lumps,)),
+            pltpu.SemaphoreType.DMA((2, lumps)),
+            pltpu.SemaphoreType.DMA((2, lumps, n // 2)),
+            pltpu.SemaphoreType.DMA((2, n // 2, lumps)),
+            pltpu.SemaphoreType.DMA((2, lumps)),
+            pltpu.SemaphoreType.DMA((lumps,)),
         ],
         compiler_params=pltpu.CompilerParams(
-            collective_id=0, has_side_effects=True, vmem_limit_bytes=56 * 1024 * 1024
+            collective_id=0, has_side_effects=True, vmem_limit_bytes=50 * 1024 * 1024
         ),
     )(
         queries, keys, values, proj_weight, residual, norm_gain.reshape(1, width),

time: 167 us -> 143 us (0.86)
  the two profiles are of different devices: /device:TPU:20 before, /device:TPU:0 now
where the time goes in v4:
time: 143 us
  Pallas kernels  134 us (94%)
  local copies, waits for them, and re-layouts  8.24 us (6%)
    pallas_call x1, Pallas kernels, layer(): pl.pallas_call(functools.partial(layer_kernel, n, m, ny), out_shape=jax.S...  134 us
    unnamed x17, local copies, waits for them, and re-layouts  8.24 us

profile of v4, /device:TPU:0, one launch (start us, length us, event | category | flops | bytes accessed | tf_op | source)
XLA Modules:
  0.0 142.6 jit_solution(9719798095405906524)
XLA Ops:
  0.0 0.0 copy-start
  0.0 1.2 copy-done
  1.2 0.0 copy-start.1
  1.2 1.0 copy-done.1
  2.3 0.0 copy-start.2
  2.3 1.0 copy-done.2
  3.3 0.0 copy-start.3
  3.3 1.0 copy-done.3
  4.4 0.0 copy-start.4
  4.4 1.0 copy-done.4
  5.4 0.0 copy-start.5
  5.4 0.7 copy-done.5
  6.1 0.0 copy-start.6
  6.1 0.7 copy-done.6
  6.8 0.0 copy-start.7
  6.8 0.7 copy-done.7
  7.5 134.4 %shard_map.109 = bf16[128,2048]{1,0:T(8,128)(2,1)S(1)} custom-call(bf16[128,2048]{1,0:T(8,128)(2,1)S(1)} %bitcast.13, bf16[128,2048]{1,0:T(8,128)(2,1)S(1)} %bitcast.14, bf16[128,2048]{1,0:T(8,128)(2,1)S(1)} %bitcast.15, bf16[256,2048]{1,0:T(8,128)(2,1)S(1)} %copy-done, bf16[128,2048]{1,0:T(8,128)(2,1)S(1)} %bitcast.16, f32[1,2048]{1,0:T(1,128)S(1)} %bitcast.17, ...), custom_call_target="tpu_custom_call" | custom-call | tf_op jit(solution)/shard_map/pallas_call | solution.py:654
  141.8 0.8 copy.13
Async XLA Ops:
  0.0 1.2 copy-start
  1.2 1.0 copy-start.1
  2.3 1.0 copy-start.2
  3.3 1.0 copy-start.3
  4.4 1.0 copy-start.4
  5.4 0.7 copy-start.5
  6.1 0.7 copy-start.6
  6.8 0.7 copy-start.7

commit v5 on v4

--- a/solution.py
+++ b/solution.py
@@ -330,7 +330,7 @@
 
     @pl.loop(1, n)
     def _(off):
-        o_copy(flipped(me, off, n)).start()
+        o_copy(flipped(me, n - off, n)).start()
 
     for off in range(1, n):
         for o in range(1, nx):

time: 143 us -> 142 us (level)
    pallas_call x1, Pallas kernels: 134 us -> 133 us  [layer(): pl.pallas_call(functools.partial(layer_kernel, n, m, ny), out_shape=jax.S...]
where the time goes in v5:
time: 142 us; the launch traced here: 141 us
  Pallas kernels  133 us (94%)
  local copies, waits for them, and re-layouts  8.24 us (6%)
    pallas_call x1, Pallas kernels, layer(): pl.pallas_call(functools.partial(layer_kernel, n, m, ny), out_shape=jax.S...  133 us
    unnamed x17, local copies, waits for them, and re-layouts  8.24 us

profile of v5, /device:TPU:0, one launch (start us, length us, event | category | flops | bytes accessed | tf_op | source)
XLA Modules:
  0.0 141.1 jit_solution(17854718158998884019)
XLA Ops:
  0.0 0.0 copy-start
  0.0 1.2 copy-done
  1.2 0.0 copy-start.1
  1.2 1.0 copy-done.1
  2.3 0.0 copy-start.2
  2.3 1.0 copy-done.2
  3.3 0.0 copy-start.3
  3.3 1.0 copy-done.3
  4.4 0.0 copy-start.4
  4.4 1.0 copy-done.4
  5.4 0.0 copy-start.5
  5.4 0.7 copy-done.5
  6.1 0.0 copy-start.6
  6.1 0.7 copy-done.6
  6.8 0.0 copy-start.7
  6.8 0.7 copy-done.7
  7.5 132.9 %shard_map.109 = bf16[128,2048]{1,0:T(8,128)(2,1)S(1)} custom-call(bf16[128,2048]{1,0:T(8,128)(2,1)S(1)} %bitcast.13, bf16[128,2048]{1,0:T(8,128)(2,1)S(1)} %bitcast.14, bf16[128,2048]{1,0:T(8,128)(2,1)S(1)} %bitcast.15, bf16[256,2048]{1,0:T(8,128)(2,1)S(1)} %copy-done, bf16[128,2048]{1,0:T(8,128)(2,1)S(1)} %bitcast.16, f32[1,2048]{1,0:T(1,128)S(1)} %bitcast.17, ...), custom_call_target="tpu_custom_call" | custom-call | tf_op jit(solution)/shard_map/pallas_call | solution.py:654
  140.3 0.8 copy.13
Async XLA Ops:
  0.0 1.2 copy-start
  1.2 1.0 copy-start.1
  2.3 1.0 copy-start.2
  3.3 1.0 copy-start.3
  4.4 1.0 copy-start.4
  5.4 0.7 copy-start.5
  6.1 0.7 copy-start.6
  6.8 0.7 copy-start.7

commit v6 on v5

--- a/solution.py
+++ b/solution.py
@@ -508,10 +508,20 @@
             upper = jnp.dot(arrived, up_ref[:, part], preferred_element_type=f32)
             hidden.append((jax.nn.silu(gate) * upper).astype(bf16))
         hidden = jnp.concatenate(hidden, axis=1)
-        for first in range(0, width, piece):
-            part = slice(first, first + piece)
+        slot = jnp.where(inner, part_of - half, nz - 1 - part_of)
+        to = jnp.where(inner, 0, ny) + rest * 2
+        for i in range(pieces):
+            part = slice(i * piece, (i + 1) * piece)
             result = jnp.dot(hidden, down_ref[:, part], preferred_element_type=f32)
             outbox[pl.ds(even, 2), :, part] = result.astype(bf16).reshape(2, capacity, piece)
+
+            @pl.when(far)
+            def _():
+                @pl.when(jnp.logical_not(local))
+                def _():
+                    via(even, slot, to, i).start()
+
+                via(odd, slot, to + 1, i).start()
 
         @pl.when(even == 0)
         def _():
@@ -529,19 +539,10 @@
 
         @pl.when(far)
         def _():
-            slot = jnp.where(inner, part_of - half, nz - 1 - part_of)
-            to = jnp.where(inner, 0, ny) + rest * 2
-
             @pl.when(local)
             def _():
                 relay_in[slot, 0] = outbox[even]
 
-            for i in range(pieces):
-                @pl.when(jnp.logical_not(local))
-                def _():
-                    via(even, slot, to, i).start()
-
-                via(odd, slot, to + 1, i).start()
 
     def picks(facts, even, odd):
         slot = lax.broadcasted_iota(jnp.int32, (rows, 2 * capacity), 1)
@@ -552,6 +553,14 @@
     def shared(facts, pick, block):
         first, second = [jnp.dot(pick[k], block, preferred_element_type=f32) for k in range(2)]
         return facts[:, 2:3] * first + facts[:, 3:4] * second
+
+    @pl.when(inner)
+    def _():
+        for slot in range(2):
+            spread = jnp.zeros((rows, rows), f32)
+            for k in range(4):
+                spread = jnp.where(row_id == k, mate_info[slot, k : k + 1, :], spread)
+            mate_cols[slot] = spread.T
 
     @pl.loop(0, span // 2)
     def _(pair):
@@ -569,10 +578,6 @@
     @pl.when(inner)
     def _():
         for slot in (1, 0):
-            spread = jnp.zeros((rows, rows), f32)
-            for k in range(4):
-                spread = jnp.where(row_id == k, mate_info[slot, k : k + 1, :], spread)
-            mate_cols[slot] = spread.T
             facts = mate_cols.at[slot]
             pick = [picks(facts, flipped(me, p * 2, n), flipped(me, p * 2 + 1, n)) for p in range(span // 2)]
             for i in range(pieces):
@@ -705,9 +710,9 @@
             pltpu.SemaphoreType.DMA((lumps,)),
             pltpu.SemaphoreType.DMA((2, lumps)),
             pltpu.SemaphoreType.DMA((2, lumps, n // 2)),
-            pltpu.SemaphoreType.DMA((2, n // 2, lumps)),
-            pltpu.SemaphoreType.DMA((2, lumps)),
-            pltpu.SemaphoreType.DMA((lumps,)),
+            pltpu.SemaphoreType.DMA((2, n // 2, 2 * lumps)),
+            pltpu.SemaphoreType.DMA((2, 2 * lumps)),
+            pltpu.SemaphoreType.DMA((2 * lumps,)),
         ],
         compiler_params=pltpu.CompilerParams(
             collective_id=0, has_side_effects=True, vmem_limit_bytes=50 * 1024 * 1024

time: 142 us -> 141 us (level)
  no operation moved by 1% of the time
where the time goes in v6:
time: 141 us
  Pallas kernels  132 us (94%)
  local copies, waits for them, and re-layouts  8.24 us (6%)
    pallas_call x1, Pallas kernels, layer(): pl.pallas_call(functools.partial(layer_kernel, n, m, ny), out_shape=jax.S...  132 us
    unnamed x17, local copies, waits for them, and re-layouts  8.24 us

profile of v6, /device:TPU:0, one launch (start us, length us, event | category | flops | bytes accessed | tf_op | source)
XLA Modules:
  0.0 140.7 jit_solution(17744767408317349878)
XLA Ops:
  0.0 0.0 copy-start
  0.0 1.2 copy-done
  1.2 0.0 copy-start.1
  1.2 1.0 copy-done.1
  2.3 0.0 copy-start.2
  2.3 1.0 copy-done.2
  3.3 0.0 copy-start.3
  3.3 1.0 copy-done.3
  4.4 0.0 copy-start.4
  4.4 1.0 copy-done.4
  5.4 0.0 copy-start.5
  5.4 0.7 copy-done.5
  6.1 0.0 copy-start.6
  6.1 0.7 copy-done.6
  6.8 0.0 copy-start.7
  6.8 0.7 copy-done.7
  7.5 132.5 %shard_map.109 = bf16[128,2048]{1,0:T(8,128)(2,1)S(1)} custom-call(bf16[128,2048]{1,0:T(8,128)(2,1)S(1)} %bitcast.13, bf16[128,2048]{1,0:T(8,128)(2,1)S(1)} %bitcast.14, bf16[128,2048]{1,0:T(8,128)(2,1)S(1)} %bitcast.15, bf16[256,2048]{1,0:T(8,128)(2,1)S(1)} %copy-done, bf16[128,2048]{1,0:T(8,128)(2,1)S(1)} %bitcast.16, f32[1,2048]{1,0:T(1,128)S(1)} %bitcast.17, ...), custom_call_target="tpu_custom_call" | custom-call | tf_op jit(solution)/shard_map/pallas_call | solution.py:659
  139.9 0.8 copy.13
Async XLA Ops:
  0.0 1.2 copy-start
  1.2 1.0 copy-start.1
  2.3 1.0 copy-start.2
  3.3 1.0 copy-start.3
  4.4 1.0 copy-start.4
  5.4 0.7 copy-start.5
  6.1 0.7 copy-start.6
  6.8 0.7 copy-start.7
